TPU v7x, 32 devices: a whole 2x2x4 slice. The times are simulated.
32 devices in a mesh: fs: 8 (over z, y), tp: 4 (over x, core).
Axes of the slice: x: 2, y: 2, z: 4, core: 2. Of those that a mesh axis runs over, the one named last changes fastest.
Arguments:
- first_map: bfloat16 [6144, 2048], P('fs', 'tp'), may hold values from -6 to 6
- second_map: bfloat16 [6144, 2048], P('fs', 'tp'), may hold values from -6 to 6
- lambda_head: float32 [16], P('tp'), may hold values from 0.3 to 0.8
- head_gain: float32 [2048], P('tp'), may hold values from 0.1 to 1.9
- cot_output: bfloat16 [6144, 4096], P('fs'), may hold values from -6 to 6
- layer_input: bfloat16 [6144, 4096], P('fs'), may hold values from -6 to 6
- cot_values: bfloat16 [6144, 2048], P('fs', 'tp'), may hold values from -16 to 16
- factor_value: bfloat16 [4096, 256], P('fs'), may hold values from -1 to 1
- factor_output: bfloat16 [4096, 256], P('fs'), may hold values from -1 to 1
- weight_value: float32 [4096, 2048], P('fs', 'tp'), may hold values from -6 to 6
- weight_output: float32 [2048, 4096], P('tp', 'fs'), may hold values from -6 to 6
- first_value: float32 [256, 2048], P('fs', 'tp'), may hold values from -6 to 6
- second_value: float32 [256, 2048], P('fs', 'tp'), may hold values from 0.05 to 1
- first_output: float32 [256, 2048], P('fs', 'tp'), may hold values from -6 to 6
- second_output: float32 [256, 2048], P('fs', 'tp'), may hold values from 0.05 to 1
Outputs:
- new_weight_value: float32 [4096, 2048], P('fs', 'tp')
- new_first_value: float32 [256, 2048], P('fs', 'tp')
- new_second_value: float32 [256, 2048], P('fs', 'tp')
- copy_value: bfloat16 [4096, 2048], P(None, 'tp')
- new_weight_output: float32 [2048, 4096], P('tp', 'fs')
- new_first_output: float32 [256, 2048], P('fs', 'tp')
- new_second_output: float32 [256, 2048], P('fs', 'tp')
- copy_output: bfloat16 [2048, 4096], P('tp')
All inputs are finite; a program needn't handle non-finite values.
Results may differ from a plain program's by a relative error of at most 0.002.
Values may be sent and summed in bfloat16 or wider, within the bound.
No kernel may reach another device: no remote copies, remote signals or barrier semaphores. Data moves between devices by JAX's collectives and lax.ppermute only.
A program may use at most 128 MiB of HBM per device.

v0:
```python
import math

import jax
import jax.numpy as jnp
from jax import lax
from jax.experimental import pallas as pl
from jax.experimental.pallas import tpu as pltpu
from jax.sharding import PartitionSpec as P


norm_epsilon = 1e-06
first_decay = 0.9
second_decay = 0.95
learn_rate = 0.1
weight_scale = 2.0**13
ratio_scale = 2.0**10


f32, bf16, f16 = jnp.float32, jnp.bfloat16, jnp.float16


SMEM = pl.BlockSpec(memory_space=pltpu.SMEM)
VMEM = pl.BlockSpec(memory_space=pltpu.VMEM)


def head_output(first_map, second_map, lambda_head, head_gain):
    heads_here = lambda_head.shape[0]
    count, cols = first_map.shape
    head_width = cols // heads_here
    parts = 8
    rows = count // parts

    def kernel(spread, first, second, gain, out):
        @pl.loop(0, parts)
        def _(p):
            span = pl.ds(pl.multiple_of(p * rows, rows), rows)
            for h in range(heads_here):
                lanes = slice(h * head_width, (h + 1) * head_width)
                differ = first[span, lanes].astype(f32) - spread[h] * second[span, lanes].astype(f32)
                mean = jnp.mean(differ * differ, -1, keepdims=True)
                scaled = differ * lax.rsqrt(mean + norm_epsilon) * gain[:, lanes]
                out[span, lanes] = scaled.astype(bf16)

    return pl.pallas_call(
        kernel,
        out_shape=jax.ShapeDtypeStruct((count, cols), bf16),
        in_specs=[SMEM, VMEM, VMEM, VMEM],
        out_specs=VMEM,
        cost_estimate=pl.CostEstimate(flops=2000 * count * cols, bytes_accessed=6 * count * cols, transcendentals=0),
        compiler_params=pltpu.CompilerParams(vmem_limit_bytes=8 * 2**20),
        name="head_output",
    )(lambda_head, first_map, second_map, head_gain[None])


def split(x):
    high = lax.reduce_precision(x, 8, 7)
    return high.astype(bf16), (x - high).astype(bf16)


def dot(a, b, dims):
    return lax.dot_general(a, b, (dims, ((), ())), preferred_element_type=f32)


def shift(x, axis, k):
    n = lax.axis_size(axis)
    return lax.ppermute(x, axis, [(i, (i + k) % n) for i in range(n)])


def swap(x, axis, bit):
    n = lax.axis_size(axis)
    return lax.ppermute(x, axis, [(i, i ^ bit) for i in range(n)])


def put(whole, block, index, dim=0):
    return lax.dynamic_update_slice_in_dim(whole, block, index, dim)


def blocks_fs(x):
    n = lax.axis_size("fs")
    half = n // 2
    me = lax.axis_index("fs")
    outer, inner = me // 2, me % 2
    line = [x] + [shift(x, "fs", 2 * k) for k in range(1, half)]
    across = [swap(block, "fs", 1) for block in line]
    places = [(outer - k) % half * 2 for k in range(half)]
    return line + across, [p + inner for p in places] + [p + 1 - inner for p in places]


def blocks_tp(x):
    t = lax.axis_size("tp")
    bit = t // 2
    found = {0: x}
    while bit:
        for r in sorted(found):
            found[r | bit] = swap(found[r], "tp", bit)
        bit //= 2
    return [found[r] for r in range(t)]


def gather_fs(x):
    n = lax.axis_size("fs")
    half = n // 2
    me = lax.axis_index("fs")
    outer, inner = me // 2, me % 2
    arrived = [x[None]] + [shift(x, "fs", 2 * k)[None] for k in range(1, half)]
    turned = arrived[:0:-1] + arrived[:1] + arrived[:0:-1]
    mine = lax.dynamic_slice_in_dim(jnp.concatenate(turned, axis=0), half - 1 - outer, half, 0)
    other = swap(mine, "fs", 1)
    lower = jnp.where(inner == 0, mine, other)
    upper = jnp.where(inner == 0, other, mine)
    return jnp.stack([lower, upper], axis=1)


def map_tokens(blocks, places, which, tokens):
    n = len(blocks)
    count, width = tokens[0].shape
    deep, part = blocks[0].shape

    def kernel(at, *refs):
        block_refs, token_refs = refs[:n], refs[n : n + 2]
        product, whole = refs[n + 2 :]
        spans = [pl.ds(pl.multiple_of(at[b] * deep, deep), deep) for b in range(n)]
        for w, held in enumerate(token_refs):

            @pl.when(at[n] == w)
            def _():
                total = jnp.zeros((count, part), f32)
                for b in range(n):
                    total += jnp.dot(held[:, spans[b]], block_refs[b][...], preferred_element_type=f32)
                product[...] = total.T

        for b in range(n):
            whole[spans[b], :] = block_refs[b][...]

    at = jnp.stack([p.astype(jnp.int32) for p in places + [which]])
    return pl.pallas_call(
        kernel,
        out_shape=(
            jax.ShapeDtypeStruct((part, count), f32),
            jax.ShapeDtypeStruct((width, part), bf16),
        ),
        in_specs=[SMEM] + [VMEM] * (n + 2),
        out_specs=(VMEM, VMEM),
        cost_estimate=pl.CostEstimate(flops=2 * count * width * 256, bytes_accessed=2 * count * width, transcendentals=0),
        compiler_params=pltpu.CompilerParams(vmem_limit_bytes=28 * 2**20),
        name="map_tokens",
    )(at, *blocks, *tokens)


def low_rank(mapped, rights):
    t, n = lax.axis_size("tp"), lax.axis_size("fs")
    part, count = mapped[0].shape
    cols = rights[0].shape[1]
    rank = part * t // 2
    rows = rank // n

    def kernel(at, *refs):
        mapped_refs, right_refs = refs[:t], refs[t : t + 2]
        keep, send, peak, both, total = refs[t + 2 :]
        for m in range(2):
            both[m] = right_refs[m][...]
        for r in range(t):
            m, h = at[r] // (t // 2), at[r] % (t // 2)
            x = mapped_refs[r][...]
            high = x.astype(bf16)
            low = (x - high.astype(f32)).astype(bf16)
            right = both[m]
            total[m, pl.ds(pl.multiple_of(h * part, part), part), :] = jnp.dot(
                high, right, preferred_element_type=f32
            ) + jnp.dot(low, right, preferred_element_type=f32)
        top = jnp.zeros((8, cols), f32)
        for m in range(2):
            tall = jnp.abs(total[m])
            top = jnp.maximum(top, jnp.max(tall.reshape(rank // 8, 8, cols), axis=0))
        peak[...] = jnp.max(top, axis=(0, 1), keepdims=True) + jnp.zeros((8, 128), f32)
        for o in range(n // 2):
            for m in range(2):
                first = pl.multiple_of((2 * o + at[t]) * rows, rows)
                keep[o, m] = total[m, pl.ds(first, rows), :]
                other = pl.multiple_of((2 * o + 1 - at[t]) * rows, rows)
                send[o, m] = total[m, pl.ds(other, rows), :]

    me = lax.axis_index("tp")
    at = jnp.stack([me ^ r for r in range(t)] + [lax.axis_index("fs") % 2]).astype(jnp.int32)
    shape = jax.ShapeDtypeStruct((n // 2, 2, rows, cols), f32)
    return pl.pallas_call(
        kernel,
        out_shape=(shape, shape, jax.ShapeDtypeStruct((8, 128), f32)),
        in_specs=[SMEM] + [VMEM] * (t + 2),
        out_specs=(VMEM, VMEM, VMEM),
        scratch_shapes=[pltpu.VMEM((2, count, cols), bf16), pltpu.VMEM((2, rank, cols), f32)],
        cost_estimate=pl.CostEstimate(flops=8 * count * rank * cols, bytes_accessed=4 * rank * cols, transcendentals=0),
        name="low_rank",
    )(at, *mapped, *rights)


def scale_of(peak):
    return jnp.clip(jnp.floor(14.0 - jnp.log2(jnp.maximum(peak, 1e-30))), -100.0, 100.0)


def pack(x, power):
    body = (x * jnp.exp2(power)).astype(f16).reshape(-1, x.shape[-1])
    return jnp.concatenate([body, jnp.full((8, x.shape[-1]), power).astype(f16)], axis=0)


def unpack(packed, shape):
    power = packed[-1, 0].astype(f32)
    return packed[:-8].astype(f32).reshape(shape) * jnp.exp2(-power), power


def add_blocks(keep, came):
    half = keep.shape[0]

    def kernel(at, a, b, *outs):
        for k in range(half):
            o = (at[0] + k) % half
            outs[k][...] = a[o] + b[o]

    at = jnp.stack([lax.axis_index("fs") // 2]).astype(jnp.int32)
    shape = jax.ShapeDtypeStruct(keep.shape[1:], f32)
    return pl.pallas_call(
        kernel,
        out_shape=(shape,) * half,
        in_specs=[SMEM, VMEM, VMEM],
        out_specs=(VMEM,) * half,
        cost_estimate=pl.CostEstimate(flops=keep.size, bytes_accessed=8 * keep.size, transcendentals=0),
        name="add_blocks",
    )(at, keep, came)


def ring_tables():
    n = lax.axis_size("fs")
    order = list(range(0, n, 2)) + list(range(n - 1, 0, -2))
    ahead = [(order[k], order[(k + 1) % n]) for k in range(n)]
    back = [(b, a) for a, b in ahead]
    return ahead, back


def ring_source(steps):
    n = lax.axis_size("fs")
    me = lax.axis_index("fs")
    place = jnp.where(me % 2 == 0, me // 2, n - 1 - me // 2)
    place = (place - steps) % n
    return jnp.where(place < n // 2, 2 * place, 2 * (n - 1 - place) + 1)


class Ring:
    def __init__(self, value, output):
        n = lax.axis_size("fs")
        self.shapes = (value.shape, output.shape)
        self.ahead, self.back = ring_tables()
        self.down = self.up = jnp.stack([value, output.reshape(value.shape)])
        self.steps = n // 2
        self.step = 0
        self.blocks = [(lax.axis_index("fs"), value, output)]

    def start(self):
        self.step += 1
        self.send()
        self.keep()

    def send(self):
        if self.step < self.steps:
            self.down = lax.ppermute(self.down, "fs", self.ahead)
            self.up = lax.ppermute(self.up, "fs", self.back)
        else:
            self.down = lax.ppermute(self.down[0], "fs", self.ahead)
            self.up = lax.ppermute(self.up[1], "fs", self.back)

    def keep(self):
        s = self.step
        if s < self.steps:
            for k, block in ((s, self.down), (-s, self.up)):
                self.blocks.append((ring_source(k), block[0], block[1].reshape(self.shapes[1])))
        else:
            self.blocks.append((ring_source(s), self.down, self.up.reshape(self.shapes[1])))

    def empty(self, after):
        n = lax.axis_size("fs")
        (rows, inner), (outer, cols) = self.shapes
        index, value, output = self.blocks[0]
        value, output, _ = lax.optimization_barrier((value, output, after))
        return (
            put(jnp.zeros((rows * n, inner), f16), value, index * rows, 0),
            put(jnp.zeros((outer, cols * n), f16), output, index * cols, 1),
        )

    def whole(self, value, output):
        rows, cols = self.shapes[0][0], self.shapes[1][1]
        for index, v, o in self.blocks[1:-1]:
            value = put(value, v, index * rows, 0)
            output = put(output, o, index * cols, 1)
        return value, output


def moments(projected, clip_factor, first_old, second_old):
    scaled = clip_factor * projected
    first_new = first_decay * first_old + (1.0 - first_decay) * scaled
    second_new = second_decay * second_old + (1.0 - second_decay) * scaled * scaled
    return first_new, second_new, first_new * lax.rsqrt(second_new)


def update(
    first_map,
    second_map,
    lambda_head,
    head_gain,
    cot_output,
    layer_input,
    cot_values,
    factor_value,
    factor_output,
    weight_value,
    weight_output,
    first_value,
    second_value,
    first_output,
    second_output,
):
    n, t = lax.axis_size("fs"), lax.axis_size("tp")
    column = lax.axis_index("tp")
    rank = factor_value.shape[1]
    part = 2 * rank // t
    half = t // 2

    first = column % half * part
    own = jnp.where(
        column < half,
        lax.dynamic_slice_in_dim(factor_value, first, part, 1),
        lax.dynamic_slice_in_dim(factor_output, first, part, 1),
    )
    blocks, places = blocks_fs(own)
    ring = Ring((weight_value * weight_scale).astype(f16), (weight_output * weight_scale).astype(f16))
    while ring.step < ring.steps:
        ring.start()
    lines, first_map, second_map = lax.optimization_barrier((blocks[: n // 2], first_map, second_map))
    blocks = lines + blocks[n // 2 :]
    heads_out = head_output(first_map, second_map, lambda_head, head_gain)
    mapped, piece = map_tokens(blocks, places, column // half, (layer_input, cot_output))
    wides = ring.empty(mapped)
    mapped = blocks_tp(mapped)
    keep, send, peak = low_rank(mapped, (cot_values, heads_out))
    peak = peak[0, 0]
    packed = pack(send, scale_of(peak))
    packed = swap(packed, "fs", 1)
    came, power = unpack(packed, send.shape)
    power = scale_of(peak + jnp.exp2(15.0 - power))
    pieces = blocks_tp(piece)
    sums = add_blocks(keep, came)
    packed = [pack(sums[k], power) for k in range(1, n // 2)]
    packed = [shift(p, "fs", 2 * (k + 1)) for k, p in enumerate(packed)]
    low = sums[0]
    for p in packed:
        low = low + unpack(p, low.shape)[0]
    square = jnp.sum(low * low)
    squares = lax.all_to_all(
        jnp.broadcast_to(square, (n * t, 1, 128)), ("fs", "tp"), 0, 0, tiled=False
    )
    pieces = jnp.stack(pieces)
    pieces = jnp.stack([pieces[column ^ c] for c in range(t)])
    pieces, squares = lax.optimization_barrier((pieces, squares))
    total = jnp.sum(squares[:, 0, 0])
    clip_factor = jnp.minimum(1.0, math.sqrt(rank * cot_values.shape[1] * t) * lax.rsqrt(total + norm_epsilon))
    first_v, second_v, ratio_value = moments(low[0], clip_factor, first_value, second_value)
    first_o, second_o, ratio_output = moments(low[1], clip_factor, first_output, second_output)

    ratio = jnp.stack([ratio_value, ratio_output]) * ratio_scale
    ratios = gather_fs(ratio.astype(f16)).reshape(n, 2, rank // n, -1).astype(f32)
    ratios = ratios * (-learn_rate / ratio_scale)

    def step(which):
        high, low = split(ratios[:, which].reshape(rank, -1))
        return jnp.concatenate([high, low], axis=0)

    step_value, step_output = step(0), step(1)

    def twice(x):
        return jnp.concatenate([x, x], axis=1)

    wide_value, wide_output = ring.whole(*wides)
    new_value = weight_value + dot(twice(factor_value), step_value, ((1,), (0,)))
    new_output = weight_output + dot(step_output, twice(factor_output), ((0,), (1,)))
    whole_value = jnp.concatenate([pieces[c] for c in range(half)] * 2, axis=1)
    whole_output = jnp.concatenate([pieces[c] for c in range(half, t)] * 2, axis=1)

    def value_rows(held, factor):
        return (held.astype(f32) * (1.0 / weight_scale) + dot(factor, step_value, ((1,), (0,)))).astype(bf16)

    def output_cols(held, factor):
        return (held.astype(f32) * (1.0 / weight_scale) + dot(step_output, factor, ((0,), (1,)))).astype(bf16)

    copy_value = value_rows(wide_value, whole_value)
    copy_output = output_cols(wide_output, whole_output)
    index, far_value, far_output = ring.blocks[-1]
    rows, cols = far_value.shape[0], far_output.shape[1]
    far_value, far_output, copy_value, copy_output = lax.optimization_barrier(
        (far_value, far_output, copy_value, copy_output)
    )

    def rows_of(factor, count):
        return lax.dynamic_slice_in_dim(factor, index * count, count, 0)

    copy_value = put(copy_value, value_rows(far_value, rows_of(whole_value, rows)), index * rows, 0)
    copy_output = put(copy_output, output_cols(far_output, rows_of(whole_output, cols)), index * cols, 1)
    return (
        new_value,
        first_v,
        second_v,
        copy_value,
        new_output,
        first_o,
        second_o,
        copy_output,
    )


def solution(mesh):
    placed = (
        P("fs", "tp"),
        P("fs", "tp"),
        P("tp"),
        P("tp"),
        P("fs", None),
        P("fs", None),
        P("fs", "tp"),
        P("fs", None),
        P("fs", None),
        P("fs", "tp"),
        P("tp", "fs"),
        P("fs", "tp"),
        P("fs", "tp"),
        P("fs", "tp"),
        P("fs", "tp"),
    )
    return jax.shard_map(
        update,
        mesh=mesh,
        in_specs=placed,
        out_specs=(
            P("fs", "tp"),
            P("fs", "tp"),
            P("fs", "tp"),
            P(None, "tp"),
            P("tp", "fs"),
            P("fs", "tp"),
            P("fs", "tp"),
            P("tp", None),
        ),
        check_vma=False,
    )
```

profile of v0, /device:TPU:0, one launch (start us, length us, event | category | flops | bytes accessed | tf_op | source)
XLA Modules:
  0.0 174.1 jit_solution(6658979721530224277)
XLA Ops:
  1.7 3.1 %collective-permute-start = (bf16[512,128]{1,0:T(8,128)(2,1)S(1)}, bf16[512,128]{1,0:T(8,128)(2,1)S(1)}, u32[]{:S(2)}, u32[]{:S(2)}) collective-permute-start(bf16[512,128]{1,0:T(8,128)(2,1)S(1)} %dynamic-slice_select_fusion.refs_0_), channel_id=1, source_target_pairs={{0,8},{4,12},{8,16},{12,20},{16,24},{20,28},{24,0},{28,4},{1,9},{5... | collective-permute-start | bytes 393224 | tf_op jit(solution)/shard_map/ppermute | solution.py:66
  4.8 2.6 %collective-permute-start.1 = (bf16[512,128]{1,0:T(8,128)(2,1)S(1)}, bf16[512,128]{1,0:T(8,128)(2,1)S(1)}, u32[]{:S(2)}, u32[]{:S(2)}) collective-permute-start(bf16[512,128]{1,0:T(8,128)(2,1)S(1)} %dynamic-slice_select_fusion.refs_0_), channel_id=1, source_target_pairs={{0,16},{4,20},{8,24},{12,28},{16,0},{20,4},{24,8},{28,12},{1,17},{... | collective-permute-start | bytes 393224 | tf_op jit(solution)/shard_map/ppermute | solution.py:66
  13.0 3.0 %collective-permute-done.1.refs_2_ = bf16[512,128]{1,0:T(8,128)(2,1)S(1)} collective-permute-done((bf16[512,128]{1,0:T(8,128)(2,1)S(1)}, bf16[512,128]{1,0:T(8,128)(2,1)S(1)}, u32[]{:S(2)}, u32[]{:S(2)}) %collective-permute-start.1) | collective-permute-done | bytes 131104 | tf_op jit(solution)/shard_map/ppermute | solution.py:66
  18.1 4.2 %collective-permute-done.5.refs_6_ = bf16[512,128]{1,0:T(8,128)(2,1)S(1)} collective-permute-done((bf16[512,128]{1,0:T(8,128)(2,1)S(1)}, bf16[512,128]{1,0:T(8,128)(2,1)S(1)}, u32[]{:S(2)}, u32[]{:S(2)}) %collective-permute-start.5) | collective-permute-done | bytes 131104 | tf_op jit(solution)/shard_map/ppermute | solution.py:71
  24.1 2.8 %copy-done = bf16[768,4096]{1,0:T(8,128)(2,1)S(1)} copy-done((bf16[768,4096]{1,0:T(8,128)(2,1)S(1)}, bf16[768,4096]{1,0:T(8,128)(2,1)}, u32[]{:S(2)}) %copy-start) | copy-done | bytes 6291480
  26.9 2.8 %copy-done.1 = bf16[768,4096]{1,0:T(8,128)(2,1)S(1)} copy-done((bf16[768,4096]{1,0:T(8,128)(2,1)S(1)}, bf16[768,4096]{1,0:T(8,128)(2,1)}, u32[]{:S(2)}) %copy-start.1) | copy-done | bytes 6291480
  29.7 2.5 %map_tokens.1 = (f32[128,768]{1,0:T(8,128)S(1)}, bf16[4096,128]{1,0:T(8,128)(2,1)S(1)}) custom-call(s32[9]{0:T(128)S(1)} %stack.111.at, bf16[512,128]{1,0:T(8,128)(2,1)S(1)} %dynamic-slice_select_fusion.refs_0_, bf16[512,128]{1,0:T(8,128)(2,1)S(1)} %collective-permute-done.refs_1_, bf16[512,128]{1,0:T(8,128)(2,1)S(1)} %collective-permute-done.1.refs_2_, ...), custom_call_target="tpu_custom_call" | custom-call | flops 1610612736 | bytes 6291456 | tf_op jit(solution)/shard_map/map_tokens/pallas_call | solution.py:136
  37.4 5.1 %collective-permute-done.11.refs_2_ = f32[128,768]{1,0:T(8,128)} collective-permute-done((f32[128,768]{1,0:T(8,128)S(1)}, f32[128,768]{1,0:T(8,128)}, u32[]{:S(2)}, u32[]{:S(2)}) %collective-permute-start.11) | collective-permute-done | bytes 393248 | tf_op jit(solution)/shard_map/ppermute | solution.py:71
  47.2 2.5 %broadcast_in_dim.32 = f16[512,4096]{1,0:T(8,128)(2,1)} broadcast(f16[]{:T(256)} %constant.223.clone.1), dimensions={} | broadcast | bytes 4194306 | tf_op jit(solution)/shard_map/broadcast_in_dim | solution.py:285
  50.6 4.0 %low_rank.1 = (f32[4,2,32,512]{3,2,1,0:T(8,128)}, f32[4,2,32,512]{3,2,1,0:T(8,128)}, f32[8,128]{1,0:T(8,128)}) custom-call(s32[5]{0:T(128)} %stack.124.at, f32[128,768]{1,0:T(8,128)} %copy-done.3, f32[128,768]{1,0:T(8,128)} %collective-permute-done.10.refs_1_, f32[128,768]{1,0:T(8,128)} %collective-permute-done.11.refs_2_, ...), custom_call_target="tpu_custom_call" | custom-call | flops 805306368 | bytes 524288 | tf_op jit(solution)/shard_map/low_rank/pallas_call | solution.py:186
  64.6 2.4 %fusion.8 = (f16[512,4096]{1,0:T(8,128)(2,1)}, f16[4096,512]{1,0:T(8,128)(2,1)}) fusion(f16[512,4096]{1,0:T(8,128)(2,1)} %constant_dynamic-update-slice_fusion.1, s32[]{:T(128)S(6)} %select_n.222, f16[2,512,512]{2,1,0:T(8,128)(2,1)} %collective-permute-done.21, f16[4096,512]{1,0:T(8,128)(2,1)} %constant_dynamic-update-slice_fusion.3), kind=kLoop, calls=%fused_computation.35 | loop fusion | bytes 2097156 | tf_op jit(solution)/shard_map/dynamic_update_slice | solution.py:75
  77.2 2.4 %fusion.7 = (f16[512,4096]{1,0:T(8,128)(2,1)}, f16[4096,512]{1,0:T(8,128)(2,1)}) fusion(f16[512,4096]{1,0:T(8,128)(2,1)} %get-tuple-element.82, s32[]{:T(128)S(6)} %select_n.225, f16[2,512,512]{2,1,0:T(8,128)(2,1)} %collective-permute-done.25, f16[4096,512]{1,0:T(8,128)(2,1)} %get-tuple-element.83), kind=kLoop, calls=%fused_computation.33 | loop fusion | bytes 2097156 | tf_op jit(solution)/shard_map/dynamic_update_slice | solution.py:75
  79.7 12.7 %collective-permute-done.14 = f16[72,512]{1,0:T(8,128)(2,1)S(1)} collective-permute-done((f16[72,512]{1,0:T(8,128)(2,1)S(1)}, f16[72,512]{1,0:T(8,128)(2,1)S(1)}, u32[]{:S(2)}, u32[]{:S(2)}) %collective-permute-start.14) | collective-permute-done | bytes 73760 | tf_op jit(solution)/shard_map/ppermute | solution.py:66
  96.0 2.4 %collective-permute-done.16 = f16[72,512]{1,0:T(8,128)(2,1)S(1)} collective-permute-done((f16[72,512]{1,0:T(8,128)(2,1)S(1)}, f16[72,512]{1,0:T(8,128)(2,1)S(1)}, u32[]{:S(2)}, u32[]{:S(2)}) %collective-permute-start.16) | collective-permute-done | bytes 73760 | tf_op jit(solution)/shard_map/ppermute | solution.py:66
  102.4 4.3 %all-to-all-start = ((f32[32,1,128]{2,1,0:T(1,128)}), f32[32,1,128]{2,1,0:T(1,128)S(1)}, u32[]{:S(2)}, u32[]{:S(2)}) async-start(f32[32,1,128]{2,1,0:T(1,128)} %broadcast_in_dim.27), calls=%async_computation | async-start | bytes 32768 | tf_op jit(solution)/shard_map/all_to_all | solution.py:356
  108.8 2.4 %fusion.6 = (f16[512,4096]{1,0:T(8,128)(2,1)}, f16[4096,512]{1,0:T(8,128)(2,1)}) fusion(f16[512,4096]{1,0:T(8,128)(2,1)} %get-tuple-element.80, s32[]{:T(128)S(6)} %select_n.228, f16[2,512,512]{2,1,0:T(8,128)(2,1)} %collective-permute-done.22, f16[4096,512]{1,0:T(8,128)(2,1)} %get-tuple-element.81), kind=kLoop, calls=%fused_computation.31 | loop fusion | bytes 2097156 | tf_op jit(solution)/shard_map/dynamic_update_slice | solution.py:75
  119.9 3.7 %collective-permute-start.17 = (f16[2,32,512]{2,1,0:T(8,128)(2,1)S(1)}, f16[2,32,512]{2,1,0:T(8,128)(2,1)S(1)}, u32[]{:S(2)}, u32[]{:S(2)}) collective-permute-start(f16[2,32,512]{2,1,0:T(8,128)(2,1)S(1)} %fusion.26), channel_id=1, source_target_pairs={{0,24},{4,28},{8,0},{12,4},{16,8},{20,12},{24,16},{28,20},{1,25},{... | collective-permute-start | bytes 196616 | tf_op jit(solution)/shard_map/ppermute | solution.py:66
  124.7 2.4 %slice_bitcast_fusion.1 = (bf16[4096,128]{1,0:T(8,128)(2,1)S(1)}, bf16[4096,128]{1,0:T(8,128)(2,1)S(1)}, bf16[4096,128]{1,0:T(8,128)(2,1)S(1)}, bf16[4096,128]{1,0:T(8,128)(2,1)S(1)}) fusion(bf16[4,4096,128]{2,1,0:T(8,128)(2,1)} %pad_maximum_fusion.1), kind=kLoop, calls=%fused_computation.12 | loop fusion | bytes 8388608 | tf_op jit(solution)/shard_map/squeeze | solution.py:384
  127.5 8.0 %collective-permute-done.17 = f16[2,32,512]{2,1,0:T(8,128)(2,1)S(1)} collective-permute-done((f16[2,32,512]{2,1,0:T(8,128)(2,1)S(1)}, f16[2,32,512]{2,1,0:T(8,128)(2,1)S(1)}, u32[]{:S(2)}, u32[]{:S(2)}) %collective-permute-start.17) | collective-permute-done | bytes 65568 | tf_op jit(solution)/shard_map/ppermute | solution.py:66
  135.5 4.7 %collective-permute-done.18 = f16[2,32,512]{2,1,0:T(8,128)(2,1)S(1)} collective-permute-done((f16[2,32,512]{2,1,0:T(8,128)(2,1)S(1)}, f16[2,32,512]{2,1,0:T(8,128)(2,1)S(1)}, u32[]{:S(2)}, u32[]{:S(2)}) %collective-permute-start.18) | collective-permute-done | bytes 65568 | tf_op jit(solution)/shard_map/ppermute | solution.py:66
  141.3 5.7 %collective-permute-done.20 = f16[4,2,32,512]{3,2,1,0:T(8,128)(2,1)S(1)} collective-permute-done((f16[4,2,32,512]{3,2,1,0:T(8,128)(2,1)S(1)}, f16[4,2,32,512]{3,2,1,0:T(8,128)(2,1)S(1)}, u32[]{:S(2)}, u32[]{:S(2)}) %collective-permute-start.20) | collective-permute-done | bytes 262176 | tf_op jit(solution)/shard_map/ppermute | solution.py:71
  153.9 4.2 %add_convert_fusion = bf16[512,4096]{1,0:T(8,128)(2,1)S(1)} fusion(f16[512,4096]{1,0:T(8,128)(2,1)} %get-tuple-element.72, bf16[256,512]{1,0:T(8,128)(2,1)S(1)} %get-tuple-element.85, bf16[256,512]{1,0:T(8,128)(2,1)S(1)} %get-tuple-element.84, bf16[4096,128]{1,0:T(8,128)(2,1)S(1)} %get-tuple-element.63, bf16[4096,128]{1,0:T(8,128)(2,1)S(1)} %get-tuple-element.62), kind=kOutput, calls=%fused_computation | convolution fusion | flops 2173698048 | bytes 11010048 | tf_op jit(solution)/shard_map/dot_general | solution.py:61
  160.5 4.3 %add_convert_fusion.1 = bf16[4096,512]{1,0:T(8,128)(2,1)S(1)} fusion(f16[4096,512]{1,0:T(8,128)(2,1)} %get-tuple-element.73, bf16[256,512]{1,0:T(8,128)(2,1)S(1)} %get-tuple-element.87, bf16[256,512]{1,0:T(8,128)(2,1)S(1)} %get-tuple-element.86, bf16[4096,128]{1,0:T(8,128)(2,1)S(1)} %get-tuple-element.64, bf16[4096,128]{1,0:T(8,128)(2,1)S(1)} %get-tuple-element.65), kind=kOutput, calls=%fused_computation.1 | convolution fusion | flops 2173698048 | bytes 11010048 | tf_op jit(solution)/shard_map/dot_general | solution.py:61
  164.8 4.8 %collective-permute-done.24 = f16[512,512]{1,0:T(8,128)(2,1)S(1)} collective-permute-done((f16[512,512]{1,0:T(8,128)(2,1)S(1)}, f16[512,512]{1,0:T(8,128)(2,1)S(1)}, u32[]{:S(2)}, u32[]{:S(2)}) %collective-permute-start.24) | collective-permute-done | bytes 524320 | tf_op jit(solution)/shard_map/ppermute | solution.py:267
  (160 shorter events, 70.7 us)
Async XLA Ops:
  1.7 9.6 %collective-permute-start = (bf16[512,128]{1,0:T(8,128)(2,1)S(1)}, bf16[512,128]{1,0:T(8,128)(2,1)S(1)}, u32[]{:S(2)}, u32[]{:S(2)}) collective-permute-start(bf16[512,128]{1,0:T(8,128)(2,1)S(1)} %dynamic-slice_select_fusion.refs_0_), channel_id=1, source_target_pairs={{0,8},{4,12},{8,16},{12,20},{16,24},{20,28},{24,0},{28,4},{1,9},{5... | collective-permute-start | bytes 393224 | tf_op jit(solution)/shard_map/ppermute | solution.py:66
  4.8 11.2 %collective-permute-start.1 = (bf16[512,128]{1,0:T(8,128)(2,1)S(1)}, bf16[512,128]{1,0:T(8,128)(2,1)S(1)}, u32[]{:S(2)}, u32[]{:S(2)}) collective-permute-start(bf16[512,128]{1,0:T(8,128)(2,1)S(1)} %dynamic-slice_select_fusion.refs_0_), channel_id=1, source_target_pairs={{0,16},{4,20},{8,24},{12,28},{16,0},{20,4},{24,8},{28,12},{1,17},{... | collective-permute-start | bytes 393224 | tf_op jit(solution)/shard_map/ppermute | solution.py:66
  7.4 10.2 %collective-permute-start.2 = (bf16[512,128]{1,0:T(8,128)(2,1)S(1)}, bf16[512,128]{1,0:T(8,128)(2,1)S(1)}, u32[]{:S(2)}, u32[]{:S(2)}) collective-permute-start(bf16[512,128]{1,0:T(8,128)(2,1)S(1)} %dynamic-slice_select_fusion.refs_0_), channel_id=1, source_target_pairs={{0,24},{4,28},{8,0},{12,4},{16,8},{20,12},{24,16},{28,20},{1,25},{... | collective-permute-start | bytes 393224 | tf_op jit(solution)/shard_map/ppermute | solution.py:66
  8.7 9.4 %collective-permute-start.3 = (bf16[512,128]{1,0:T(8,128)(2,1)S(1)}, bf16[512,128]{1,0:T(8,128)(2,1)S(1)}, u32[]{:S(2)}, u32[]{:S(2)}) collective-permute-start(bf16[512,128]{1,0:T(8,128)(2,1)S(1)} %dynamic-slice_select_fusion.refs_0_), channel_id=1, source_target_pairs={{0,4},{4,0},{8,12},{12,8},{16,20},{20,16},{24,28},{28,24},{1,5},{5... | collective-permute-start | bytes 393224 | tf_op jit(solution)/shard_map/ppermute | solution.py:71
  32.2 10.3 %collective-permute-start.11 = (f32[128,768]{1,0:T(8,128)S(1)}, f32[128,768]{1,0:T(8,128)}, u32[]{:S(2)}, u32[]{:S(2)}) collective-permute-start(f32[128,768]{1,0:T(8,128)S(1)} %get-tuple-element.36.refs_0_), channel_id=1, source_target_pairs={{0,2},{1,3},{2,0},{3,1},{4,6},{5,7},{6,4},{7,5},{8,10},{9,11},{10,... | collective-permute-start | bytes 1179656 | tf_op jit(solution)/shard_map/ppermute | solution.py:71
  35.3 27.2 %collective-permute-start.21 = (f16[2,512,512]{2,1,0:T(8,128)(2,1)}, f16[2,512,512]{2,1,0:T(8,128)(2,1)}, u32[]{:S(2)}, u32[]{:S(2)}) collective-permute-start(f16[2,512,512]{2,1,0:T(8,128)(2,1)} %pad_maximum_fusion.4), channel_id=1, source_target_pairs={{0,8},{8,16},{16,24},{24,28},{28,20},{20,12},{12,4},{4,0},{1,9},{9... | collective-permute-start | bytes 3145736 | tf_op jit(solution)/shard_map/ppermute | solution.py:264
  37.3 26.9 %collective-permute-start.25 = (f16[2,512,512]{2,1,0:T(8,128)(2,1)}, f16[2,512,512]{2,1,0:T(8,128)(2,1)}, u32[]{:S(2)}, u32[]{:S(2)}) collective-permute-start(f16[2,512,512]{2,1,0:T(8,128)(2,1)} %pad_maximum_fusion.4), channel_id=1, source_target_pairs={{8,0},{16,8},{24,16},{28,24},{20,28},{12,20},{4,12},{0,4},{9,1},{1... | collective-permute-start | bytes 3145736 | tf_op jit(solution)/shard_map/ppermute | solution.py:265
  37.4 13.3 %collective-permute-start.10 = (f32[128,768]{1,0:T(8,128)S(1)}, f32[128,768]{1,0:T(8,128)}, u32[]{:S(2)}, u32[]{:S(2)}) collective-permute-start(f32[128,768]{1,0:T(8,128)S(1)} %get-tuple-element.36.refs_0_), channel_id=1, source_target_pairs={{0,1},{1,0},{2,3},{3,2},{4,5},{5,4},{6,7},{7,6},{8,9},{9,8},{10,11... | collective-permute-start | bytes 1179656 | tf_op jit(solution)/shard_map/ppermute | solution.py:71
  45.7 33.9 %collective-permute-start.8 = (bf16[4096,128]{1,0:T(8,128)(2,1)S(1)}, bf16[4096,128]{1,0:T(8,128)(2,1)}, u32[]{:S(2)}, u32[]{:S(2)}) collective-permute-start(bf16[4096,128]{1,0:T(8,128)(2,1)S(1)} %get-tuple-element.35), channel_id=1, source_target_pairs={{0,2},{1,3},{2,0},{3,1},{4,6},{5,7},{6,4},{7,5},{8,10},{9,11},{10,... | collective-permute-start | bytes 3145736 | tf_op jit(solution)/shard_map/ppermute | solution.py:71
  57.8 9.4 %collective-permute-start.13 = (f16[264,512]{1,0:T(8,128)(2,1)S(1)}, f16[264,512]{1,0:T(8,128)(2,1)S(1)}, u32[]{:S(2)}, u32[]{:S(2)}) collective-permute-start(f16[264,512]{1,0:T(8,128)(2,1)S(1)} %concatenate.41), channel_id=1, source_target_pairs={{0,4},{4,0},{8,12},{12,8},{16,20},{20,16},{24,28},{28,24},{1,5},{5... | collective-permute-start | bytes 811016 | tf_op jit(solution)/shard_map/ppermute | solution.py:71
  62.6 44.2 %collective-permute-start.22 = (f16[2,512,512]{2,1,0:T(8,128)(2,1)}, f16[2,512,512]{2,1,0:T(8,128)(2,1)}, u32[]{:S(2)}, u32[]{:S(2)}) collective-permute-start(f16[2,512,512]{2,1,0:T(8,128)(2,1)} %collective-permute-done.21), channel_id=1, source_target_pairs={{0,8},{8,16},{16,24},{24,28},{28,20},{20,12},{12,4},{4,0},{1,9},{9... | collective-permute-start | bytes 3145736 | tf_op jit(solution)/shard_map/ppermute | solution.py:264
  64.2 44.4 %collective-permute-start.26 = (f16[2,512,512]{2,1,0:T(8,128)(2,1)}, f16[2,512,512]{2,1,0:T(8,128)(2,1)}, u32[]{:S(2)}, u32[]{:S(2)}) collective-permute-start(f16[2,512,512]{2,1,0:T(8,128)(2,1)} %collective-permute-done.25), channel_id=1, source_target_pairs={{8,0},{16,8},{24,16},{28,24},{20,28},{12,20},{4,12},{0,4},{9,1},{1... | collective-permute-start | bytes 3145736 | tf_op jit(solution)/shard_map/ppermute | solution.py:265
  73.1 19.4 %collective-permute-start.14 = (f16[72,512]{1,0:T(8,128)(2,1)S(1)}, f16[72,512]{1,0:T(8,128)(2,1)S(1)}, u32[]{:S(2)}, u32[]{:S(2)}) collective-permute-start(f16[72,512]{1,0:T(8,128)(2,1)S(1)} %concatenate.42), channel_id=1, source_target_pairs={{0,8},{4,12},{8,16},{12,20},{16,24},{20,28},{24,0},{28,4},{1,9},{5... | collective-permute-start | bytes 221192 | tf_op jit(solution)/shard_map/ppermute | solution.py:66
  75.5 18.1 %collective-permute-start.15 = (f16[72,512]{1,0:T(8,128)(2,1)S(1)}, f16[72,512]{1,0:T(8,128)(2,1)S(1)}, u32[]{:S(2)}, u32[]{:S(2)}) collective-permute-start(f16[72,512]{1,0:T(8,128)(2,1)S(1)} %concatenate.43), channel_id=1, source_target_pairs={{0,16},{4,20},{8,24},{12,28},{16,0},{20,4},{24,8},{28,12},{1,17},{... | collective-permute-start | bytes 221192 | tf_op jit(solution)/shard_map/ppermute | solution.py:66
  79.6 34.0 %collective-permute-start.7 = (bf16[4096,128]{1,0:T(8,128)(2,1)S(1)}, bf16[4096,128]{1,0:T(8,128)(2,1)}, u32[]{:S(2)}, u32[]{:S(2)}) collective-permute-start(bf16[4096,128]{1,0:T(8,128)(2,1)S(1)} %get-tuple-element.35), channel_id=1, source_target_pairs={{0,1},{1,0},{2,3},{3,2},{4,5},{5,4},{6,7},{7,6},{8,9},{9,8},{10,11... | collective-permute-start | bytes 3145736 | tf_op jit(solution)/shard_map/ppermute | solution.py:71
  92.4 21.2 %collective-permute-start.9 = (bf16[4096,128]{1,0:T(8,128)(2,1)}, bf16[4096,128]{1,0:T(8,128)(2,1)}, u32[]{:S(2)}, u32[]{:S(2)}) collective-permute-start(bf16[4096,128]{1,0:T(8,128)(2,1)} %collective-permute-done.8), channel_id=1, source_target_pairs={{0,1},{1,0},{2,3},{3,2},{4,5},{5,4},{6,7},{7,6},{8,9},{9,8},{10,11... | collective-permute-start | bytes 3145736 | tf_op jit(solution)/shard_map/ppermute | solution.py:71
  102.4 15.9 %all-to-all-start = ((f32[32,1,128]{2,1,0:T(1,128)}), f32[32,1,128]{2,1,0:T(1,128)S(1)}, u32[]{:S(2)}, u32[]{:S(2)}) async-start(f32[32,1,128]{2,1,0:T(1,128)} %broadcast_in_dim.27), calls=%async_computation | async-start | bytes 32768 | tf_op jit(solution)/shard_map/all_to_all | solution.py:356
  106.8 44.8 %collective-permute-start.23 = (f16[2,512,512]{2,1,0:T(8,128)(2,1)}, f16[2,512,512]{2,1,0:T(8,128)(2,1)S(1)}, u32[]{:S(2)}, u32[]{:S(2)}) collective-permute-start(f16[2,512,512]{2,1,0:T(8,128)(2,1)} %collective-permute-done.22), channel_id=1, source_target_pairs={{0,8},{8,16},{16,24},{24,28},{28,20},{20,12},{12,4},{4,0},{1,9},{9... | collective-permute-start | bytes 3145736 | tf_op jit(solution)/shard_map/ppermute | solution.py:264
  108.6 44.2 %collective-permute-start.27 = (f16[2,512,512]{2,1,0:T(8,128)(2,1)}, f16[2,512,512]{2,1,0:T(8,128)(2,1)S(1)}, u32[]{:S(2)}, u32[]{:S(2)}) collective-permute-start(f16[2,512,512]{2,1,0:T(8,128)(2,1)} %collective-permute-done.26), channel_id=1, source_target_pairs={{8,0},{16,8},{24,16},{28,24},{20,28},{12,20},{4,12},{0,4},{9,1},{1... | collective-permute-start | bytes 3145736 | tf_op jit(solution)/shard_map/ppermute | solution.py:265
  119.9 15.6 %collective-permute-start.17 = (f16[2,32,512]{2,1,0:T(8,128)(2,1)S(1)}, f16[2,32,512]{2,1,0:T(8,128)(2,1)S(1)}, u32[]{:S(2)}, u32[]{:S(2)}) collective-permute-start(f16[2,32,512]{2,1,0:T(8,128)(2,1)S(1)} %fusion.26), channel_id=1, source_target_pairs={{0,24},{4,28},{8,0},{12,4},{16,8},{20,12},{24,16},{28,20},{1,25},{... | collective-permute-start | bytes 196616 | tf_op jit(solution)/shard_map/ppermute | solution.py:66
  123.6 16.6 %collective-permute-start.18 = (f16[2,32,512]{2,1,0:T(8,128)(2,1)S(1)}, f16[2,32,512]{2,1,0:T(8,128)(2,1)S(1)}, u32[]{:S(2)}, u32[]{:S(2)}) collective-permute-start(f16[2,32,512]{2,1,0:T(8,128)(2,1)S(1)} %fusion.26), channel_id=1, source_target_pairs={{0,16},{4,20},{8,24},{12,28},{16,0},{20,4},{24,8},{28,12},{1,17},{... | collective-permute-start | bytes 196616 | tf_op jit(solution)/shard_map/ppermute | solution.py:66
  123.6 16.7 %collective-permute-start.19 = (f16[2,32,512]{2,1,0:T(8,128)(2,1)S(1)}, f16[2,32,512]{2,1,0:T(8,128)(2,1)S(1)}, u32[]{:S(2)}, u32[]{:S(2)}) collective-permute-start(f16[2,32,512]{2,1,0:T(8,128)(2,1)S(1)} %fusion.26), channel_id=1, source_target_pairs={{0,8},{4,12},{8,16},{12,20},{16,24},{20,28},{24,0},{28,4},{1,9},{5... | collective-permute-start | bytes 196616 | tf_op jit(solution)/shard_map/ppermute | solution.py:66
  158.3 11.3 %collective-permute-start.24 = (f16[512,512]{1,0:T(8,128)(2,1)S(1)}, f16[512,512]{1,0:T(8,128)(2,1)S(1)}, u32[]{:S(2)}, u32[]{:S(2)}) collective-permute-start(f16[512,512]{1,0:T(8,128)(2,1)S(1)} %slice_bitcast_fusion.15), channel_id=1, source_target_pairs={{0,8},{8,16},{16,24},{24,28},{28,20},{20,12},{12,4},{4,0},{1,9},{9... | collective-permute-start | bytes 1572872 | tf_op jit(solution)/shard_map/ppermute | solution.py:267
  158.4 11.4 %collective-permute-start.28 = (f16[512,512]{1,0:T(8,128)(2,1)S(1)}, f16[512,512]{1,0:T(8,128)(2,1)S(1)}, u32[]{:S(2)}, u32[]{:S(2)}) collective-permute-start(f16[512,512]{1,0:T(8,128)(2,1)S(1)} %slice_bitcast_fusion.14), channel_id=1, source_target_pairs={{8,0},{16,8},{24,16},{28,24},{20,28},{12,20},{4,12},{0,4},{9,1},{1... | collective-permute-start | bytes 1572872 | tf_op jit(solution)/shard_map/ppermute | solution.py:268
  (32 other events, 180.9 us)
where the time goes:
time: 175 us; the launch traced here: 174 us
  waiting for transfers between devices  54 us (31%)
  starting transfers between devices  39.2 us (22%)
  local copies, waits for them, and re-layouts  37.4 us (21%)
  other arithmetic  14.6 us (8%)
  matrix products  12.3 us (7%)
  Pallas kernels  10.2 us (6%)
  between operations  6.32 us (4%)
    ppermute x9, waiting for transfers between devices, shift(): return lax.ppermute(x, axis, [(i, (i + k) % n) for i in range(n)])  31.9 us
    ppermute x12, waiting for transfers between devices, swap(): return lax.ppermute(x, axis, [(i, i ^ bit) for i in range(n)])  17.1 us
    ppermute x9, starting transfers between devices, shift(): return lax.ppermute(x, axis, [(i, (i + k) % n) for i in range(n)])  16 us
    dynamic_update_slice x8, local copies, waits for them, and re-layouts, put(): return lax.dynamic_update_slice_in_dim(whole, block, index, dim)  13.6 us
    dot_general x6, matrix products, dot(): return lax.dot_general(a, b, (dims, ((), ())), preferred_element_type=f32)  12.3 us
    ppermute x12, starting transfers between devices, swap(): return lax.ppermute(x, axis, [(i, i ^ bit) for i in range(n)])  10.6 us
    unnamed x57, local copies, waits for them, and re-layouts  10.5 us
    ppermute x3, starting transfers between devices, send(): self.down = lax.ppermute(self.down, 'fs', self.ahead)  5.42 us
  transfers between devices with their start and end apart: 30, of which 13 were waited for; matrix products, arithmetic and copies ran while one was open for 27% of the time, Pallas kernels for 4%

commit v1 on v0

--- a/solution.py
+++ b/solution.py
@@ -21,6 +21,7 @@
 
 SMEM = pl.BlockSpec(memory_space=pltpu.SMEM)
 VMEM = pl.BlockSpec(memory_space=pltpu.VMEM)
+ANY = pl.BlockSpec(memory_space=pl.ANY)
 
 
 def head_output(first_map, second_map, lambda_head, head_gain):
@@ -116,40 +117,51 @@
     count, width = tokens[0].shape
     deep, part = blocks[0].shape
 
+    parts = 4
+    rows = count // parts
+
     def kernel(at, *refs):
         block_refs, token_refs = refs[:n], refs[n : n + 2]
-        product, whole = refs[n + 2 :]
+        product, whole, held, sems = refs[n + 2 :]
         spans = [pl.ds(pl.multiple_of(at[b] * deep, deep), deep) for b in range(n)]
-        for w, held in enumerate(token_refs):
+
+        def fetch(source, p):
+            here = pl.ds(p * rows, rows)
+            return pltpu.make_async_copy(source.at[here], held.at[here], sems.at[p])
+
+        for w in range(2):
 
             @pl.when(at[n] == w)
             def _():
-                total = jnp.zeros((count, part), f32)
-                for b in range(n):
-                    total += jnp.dot(held[:, spans[b]], block_refs[b][...], preferred_element_type=f32)
-                product[...] = total.T
+                for p in range(parts):
+                    fetch(token_refs[w], p).start()
 
         for b in range(n):
             whole[spans[b], :] = block_refs[b][...]
+        for p in range(parts):
+            fetch(token_refs[0], p).wait()
+            here = slice(p * rows, (p + 1) * rows)
+            total = jnp.dot(held[here], whole[...], preferred_element_type=f32)
+            product[here, :] = total
 
     at = jnp.stack([p.astype(jnp.int32) for p in places + [which]])
     return pl.pallas_call(
         kernel,
         out_shape=(
-            jax.ShapeDtypeStruct((part, count), f32),
+            jax.ShapeDtypeStruct((count, part), f32),
             jax.ShapeDtypeStruct((width, part), bf16),
         ),
-        in_specs=[SMEM] + [VMEM] * (n + 2),
+        in_specs=[SMEM] + [VMEM] * n + [ANY] * 2,
         out_specs=(VMEM, VMEM),
+        scratch_shapes=[pltpu.VMEM((count, width), bf16), pltpu.SemaphoreType.DMA((parts,))],
         cost_estimate=pl.CostEstimate(flops=2 * count * width * 256, bytes_accessed=2 * count * width, transcendentals=0),
-        compiler_params=pltpu.CompilerParams(vmem_limit_bytes=28 * 2**20),
         name="map_tokens",
     )(at, *blocks, *tokens)
 
 
 def low_rank(mapped, rights):
     t, n = lax.axis_size("tp"), lax.axis_size("fs")
-    part, count = mapped[0].shape
+    count, part = mapped[0].shape
     cols = rights[0].shape[1]
     rank = part * t // 2
     rows = rank // n
@@ -161,7 +173,7 @@
             both[m] = right_refs[m][...]
         for r in range(t):
             m, h = at[r] // (t // 2), at[r] % (t // 2)
-            x = mapped_refs[r][...]
+            x = mapped_refs[r][...].T
             high = x.astype(bf16)
             low = (x - high.astype(f32)).astype(bf16)
             right = both[m]
@@ -172,7 +184,7 @@
         for m in range(2):
             tall = jnp.abs(total[m])
             top = jnp.maximum(top, jnp.max(tall.reshape(rank // 8, 8, cols), axis=0))
-        peak[...] = jnp.max(top, axis=(0, 1), keepdims=True) + jnp.zeros((8, 128), f32)
+        peak[...] = jnp.max(top, axis=(0, 1), keepdims=True) + jnp.zeros((8, cols), f32)
         for o in range(n // 2):
             for m in range(2):
                 first = pl.multiple_of((2 * o + at[t]) * rows, rows)
@@ -185,7 +197,7 @@
     shape = jax.ShapeDtypeStruct((n // 2, 2, rows, cols), f32)
     return pl.pallas_call(
         kernel,
-        out_shape=(shape, shape, jax.ShapeDtypeStruct((8, 128), f32)),
+        out_shape=(shape, shape, jax.ShapeDtypeStruct((8, cols), f32)),
         in_specs=[SMEM] + [VMEM] * (t + 2),
         out_specs=(VMEM, VMEM, VMEM),
         scratch_shapes=[pltpu.VMEM((2, count, cols), bf16), pltpu.VMEM((2, rank, cols), f32)],
@@ -199,13 +211,13 @@
 
 
 def pack(x, power):
-    body = (x * jnp.exp2(power)).astype(f16).reshape(-1, x.shape[-1])
-    return jnp.concatenate([body, jnp.full((8, x.shape[-1]), power).astype(f16)], axis=0)
+    body = (x.reshape(-1, x.shape[-1]) * jnp.exp2(power[:1])).astype(f16)
+    return jnp.concatenate([body, power.astype(f16)], axis=0)
 
 
 def unpack(packed, shape):
-    power = packed[-1, 0].astype(f32)
-    return packed[:-8].astype(f32).reshape(shape) * jnp.exp2(-power), power
+    power = packed[-8:].astype(f32)
+    return (packed[:-8].astype(f32) * jnp.exp2(-power[:1])).reshape(shape), power
 
 
 def add_blocks(keep, came):
@@ -337,12 +349,11 @@
     blocks = lines + blocks[n // 2 :]
     heads_out = head_output(first_map, second_map, lambda_head, head_gain)
     mapped, piece = map_tokens(blocks, places, column // half, (layer_input, cot_output))
-    wides = ring.empty(mapped)
     mapped = blocks_tp(mapped)
     keep, send, peak = low_rank(mapped, (cot_values, heads_out))
-    peak = peak[0, 0]
     packed = pack(send, scale_of(peak))
     packed = swap(packed, "fs", 1)
+    wides = ring.empty(peak)
     came, power = unpack(packed, send.shape)
     power = scale_of(peak + jnp.exp2(15.0 - power))
     pieces = blocks_tp(piece)
@@ -389,19 +400,19 @@
     def output_cols(held, factor):
         return (held.astype(f32) * (1.0 / weight_scale) + dot(step_output, factor, ((0,), (1,)))).astype(bf16)
 
-    copy_value = value_rows(wide_value, whole_value)
-    copy_output = output_cols(wide_output, whole_output)
+    def rows_of(factor, count):
+        return lax.dynamic_slice_in_dim(factor, index * count, count, 0)
+
     index, far_value, far_output = ring.blocks[-1]
     rows, cols = far_value.shape[0], far_output.shape[1]
-    far_value, far_output, copy_value, copy_output = lax.optimization_barrier(
-        (far_value, far_output, copy_value, copy_output)
-    )
-
-    def rows_of(factor, count):
-        return lax.dynamic_slice_in_dim(factor, index * count, count, 0)
-
-    copy_value = put(copy_value, value_rows(far_value, rows_of(whole_value, rows)), index * rows, 0)
-    copy_output = put(copy_output, output_cols(far_output, rows_of(whole_output, cols)), index * cols, 1)
+    copy_output = output_cols(wide_output, whole_output)
+    far_output, copy_output = lax.optimization_barrier((far_output, copy_output))
+    far_output = output_cols(far_output, rows_of(whole_output, cols))
+    copy_output = put(copy_output, far_output, index * cols, 1)
+    copy_value = value_rows(wide_value, whole_value)
+    far_value, copy_value = lax.optimization_barrier((far_value, copy_value))
+    far_value = value_rows(far_value, rows_of(whole_value, rows))
+    copy_value = put(copy_value, far_value, index * rows, 0)
     return (
         new_value,
         first_v,

time: 175 us -> 184 us (1.051)
  waiting for transfers between devices: 54 us -> 74.8 us
  local copies, waits for them, and re-layouts: 37.4 us -> 29.4 us
  starting transfers between devices: 39.2 us -> 34.9 us
  between operations: 6.32 us -> 2.02 us
  Pallas kernels: 10.2 us -> 13.5 us
  other arithmetic: 14.6 us -> 16.7 us
    ppermute x9, waiting for transfers between devices: 31.9 us -> 43.2 us  [shift(): return lax.ppermute(x, axis, [(i, (i + k) % n) for i in range(n)])]
    ppermute x3, waiting for transfers between devices: 0.01 us -> 4.68 us  [send(): self.down = lax.ppermute(self.down, 'fs', self.ahead)]
    ppermute x1, waiting for transfers between devices: 0.26 us -> 4.76 us  [send(): self.up = lax.ppermute(self.up[1], 'fs', self.back)]
    unnamed x57 -> x65, local copies, waits for them, and re-layouts: 10.5 us -> 6.34 us
    ppermute x9, starting transfers between devices: 16 us -> 12.1 us  [shift(): return lax.ppermute(x, axis, [(i, (i + k) % n) for i in range(n)])]
    ppermute x12, waiting for transfers between devices: 17.1 us -> 20.9 us  [swap(): return lax.ppermute(x, axis, [(i, i ^ bit) for i in range(n)])]
    ppermute x1, waiting for transfers between devices: 4.83 us -> 1.21 us  [send(): self.down = lax.ppermute(self.down[0], 'fs', self.ahead)]
    pallas_call x1, Pallas kernels: 2.47 us -> 5.76 us  [map_tokens(): pl.pallas_call(kernel, out_shape=(jax.ShapeDtypeStruct((count, part), f32...]
  transfers between devices with their start and end apart: 30 -> 30, of which waited for: 13 -> 15; matrix products, arithmetic and copies ran while one was open for 27% -> 25% of each run, Pallas kernels for 4% -> 4%
where the time goes in v1:
time: 184 us
  waiting for transfers between devices  74.8 us (41%)
  starting transfers between devices  34.9 us (19%)
  local copies, waits for them, and re-layouts  29.4 us (16%)
  other arithmetic  16.7 us (9%)
  Pallas kernels  13.5 us (7%)
  matrix products  12.3 us (7%)
  between operations  2.02 us (1%)
    ppermute x9, waiting for transfers between devices, shift(): return lax.ppermute(x, axis, [(i, (i + k) % n) for i in range(n)])  43.2 us
    ppermute x12, waiting for transfers between devices, swap(): return lax.ppermute(x, axis, [(i, i ^ bit) for i in range(n)])  20.9 us
    dynamic_update_slice x8, local copies, waits for them, and re-layouts, put(): return lax.dynamic_update_slice_in_dim(whole, block, index, dim)  12.4 us
    dot_general x6, matrix products, dot(): return lax.dot_general(a, b, (dims, ((), ())), preferred_element_type=f32)  12.3 us
    ppermute x9, starting transfers between devices, shift(): return lax.ppermute(x, axis, [(i, (i + k) % n) for i in range(n)])  12.1 us
    ppermute x12, starting transfers between devices, swap(): return lax.ppermute(x, axis, [(i, i ^ bit) for i in range(n)])  10.7 us
    unnamed x65, local copies, waits for them, and re-layouts  6.34 us
    pallas_call x1, Pallas kernels, map_tokens(): pl.pallas_call(kernel, out_shape=(jax.ShapeDtypeStruct((count, part), f32...  5.76 us
  transfers between devices with their start and end apart: 30, of which 15 were waited for; matrix products, arithmetic and copies ran while one was open for 25% of the time, Pallas kernels for 4%

profile of v1, /device:TPU:0, one launch (start us, length us, event | category | flops | bytes accessed | tf_op | source)
XLA Modules:
  0.0 183.6 jit_solution(17399886771403639742)
XLA Ops:
  1.7 3.1 %collective-permute-start = (bf16[512,128]{1,0:T(8,128)(2,1)S(1)}, bf16[512,128]{1,0:T(8,128)(2,1)S(1)}, u32[]{:S(2)}, u32[]{:S(2)}) collective-permute-start(bf16[512,128]{1,0:T(8,128)(2,1)S(1)} %dynamic-slice_select_fusion.refs_0_), channel_id=1, source_target_pairs={{0,8},{4,12},{8,16},{12,20},{16,24},{20,28},{24,0},{28,4},{1,9},{5... | collective-permute-start | bytes 393224 | tf_op jit(solution)/shard_map/ppermute | solution.py:67
  4.8 2.6 %collective-permute-start.1 = (bf16[512,128]{1,0:T(8,128)(2,1)S(1)}, bf16[512,128]{1,0:T(8,128)(2,1)S(1)}, u32[]{:S(2)}, u32[]{:S(2)}) collective-permute-start(bf16[512,128]{1,0:T(8,128)(2,1)S(1)} %dynamic-slice_select_fusion.refs_0_), channel_id=1, source_target_pairs={{0,16},{4,20},{8,24},{12,28},{16,0},{20,4},{24,8},{28,12},{1,17},{... | collective-permute-start | bytes 393224 | tf_op jit(solution)/shard_map/ppermute | solution.py:67
  13.0 3.0 %collective-permute-done.1.refs_2_ = bf16[512,128]{1,0:T(8,128)(2,1)S(1)} collective-permute-done((bf16[512,128]{1,0:T(8,128)(2,1)S(1)}, bf16[512,128]{1,0:T(8,128)(2,1)S(1)}, u32[]{:S(2)}, u32[]{:S(2)}) %collective-permute-start.1) | collective-permute-done | bytes 131104 | tf_op jit(solution)/shard_map/ppermute | solution.py:67
  18.7 3.6 %collective-permute-done.5.refs_6_ = bf16[512,128]{1,0:T(8,128)(2,1)S(1)} collective-permute-done((bf16[512,128]{1,0:T(8,128)(2,1)S(1)}, bf16[512,128]{1,0:T(8,128)(2,1)S(1)}, u32[]{:S(2)}, u32[]{:S(2)}) %collective-permute-start.5) | collective-permute-done | bytes 131104 | tf_op jit(solution)/shard_map/ppermute | solution.py:72
  24.8 5.8 %map_tokens.1 = (f32[768,128]{1,0:T(8,128)}, bf16[4096,128]{1,0:T(8,128)(2,1)}) custom-call(s32[9]{0:T(128)} %stack.111.at, bf16[512,128]{1,0:T(8,128)(2,1)} %copy-done.9, bf16[512,128]{1,0:T(8,128)(2,1)} %copy-done.16, bf16[512,128]{1,0:T(8,128)(2,1)} %copy-done.17, bf16[512,128]{1,0:T(8,128)(2,1)} %copy-done.18, bf16[512,128]{1,0:T(8,128)(2,1)} %copy-done.19, ...), custom_call_target="tpu_custom_call" | custom-call | flops 1610612736 | bytes 6291456 | tf_op jit(solution)/shard_map/map_tokens/pallas_call | solution.py:148
  32.2 8.8 %collective-permute-done.11.refs_2_ = f32[768,128]{1,0:T(8,128)S(1)} collective-permute-done((f32[768,128]{1,0:T(8,128)}, f32[768,128]{1,0:T(8,128)S(1)}, u32[]{:S(2)}, u32[]{:S(2)}) %collective-permute-start.11) | collective-permute-done | bytes 393248 | tf_op jit(solution)/shard_map/ppermute | solution.py:72
  51.7 4.0 %low_rank.1 = (f32[4,2,32,512]{3,2,1,0:T(8,128)}, f32[4,2,32,512]{3,2,1,0:T(8,128)}, f32[8,512]{1,0:T(8,128)}) custom-call(s32[5]{0:T(128)} %stack.124.at, f32[768,128]{1,0:T(8,128)} %get-tuple-element.36.refs_0_, f32[768,128]{1,0:T(8,128)} %copy-done.11, f32[768,128]{1,0:T(8,128)} %copy-done.10, f32[768,128]{1,0:T(8,128)} %collective-permute-done.12.refs_3_, ...), custom_call_target="tpu_custom_call" | custom-call | flops 805306368 | bytes 524288 | tf_op jit(solution)/shard_map/low_rank/pallas_call | solution.py:198
  59.3 2.5 %broadcast_in_dim.28 = f16[512,4096]{1,0:T(8,128)(2,1)} broadcast(f16[]{:T(256)} %constant.217.clone.1), dimensions={} | broadcast | bytes 4194306 | tf_op jit(solution)/shard_map/broadcast_in_dim | solution.py:297
  65.9 4.7 %collective-permute-done.21 = f16[2,512,512]{2,1,0:T(8,128)(2,1)} collective-permute-done((f16[2,512,512]{2,1,0:T(8,128)(2,1)}, f16[2,512,512]{2,1,0:T(8,128)(2,1)}, u32[]{:S(2)}, u32[]{:S(2)}) %collective-permute-start.21) | collective-permute-done | bytes 1048608 | tf_op jit(solution)/shard_map/ppermute | solution.py:276
  72.6 2.4 %fusion.8 = (f16[512,4096]{1,0:T(8,128)(2,1)}, f16[4096,512]{1,0:T(8,128)(2,1)}) fusion(f16[512,4096]{1,0:T(8,128)(2,1)} %constant_dynamic-update-slice_fusion.1, s32[]{:T(128)S(6)} %select_n.222, f16[2,512,512]{2,1,0:T(8,128)(2,1)} %collective-permute-done.21, f16[4096,512]{1,0:T(8,128)(2,1)} %constant_dynamic-update-slice_fusion.3), kind=kLoop, calls=%fused_computation.35 | loop fusion | bytes 2097156 | tf_op jit(solution)/shard_map/dynamic_update_slice | solution.py:76
  80.4 2.4 %fusion.7 = (f16[512,4096]{1,0:T(8,128)(2,1)}, f16[4096,512]{1,0:T(8,128)(2,1)}) fusion(f16[512,4096]{1,0:T(8,128)(2,1)} %get-tuple-element.82, s32[]{:T(128)S(6)} %select_n.225, f16[2,512,512]{2,1,0:T(8,128)(2,1)} %collective-permute-done.25, f16[4096,512]{1,0:T(8,128)(2,1)} %get-tuple-element.83), kind=kLoop, calls=%fused_computation.33 | loop fusion | bytes 2097156 | tf_op jit(solution)/shard_map/dynamic_update_slice | solution.py:76
  82.8 15.7 %collective-permute-done.14 = f16[72,512]{1,0:T(8,128)(2,1)S(1)} collective-permute-done((f16[72,512]{1,0:T(8,128)(2,1)S(1)}, f16[72,512]{1,0:T(8,128)(2,1)S(1)}, u32[]{:S(2)}, u32[]{:S(2)}) %collective-permute-start.14) | collective-permute-done | bytes 73760 | tf_op jit(solution)/shard_map/ppermute | solution.py:67
  98.5 6.0 %collective-permute-done.15 = f16[72,512]{1,0:T(8,128)(2,1)S(1)} collective-permute-done((f16[72,512]{1,0:T(8,128)(2,1)S(1)}, f16[72,512]{1,0:T(8,128)(2,1)S(1)}, u32[]{:S(2)}, u32[]{:S(2)}) %collective-permute-start.15) | collective-permute-done | bytes 73760 | tf_op jit(solution)/shard_map/ppermute | solution.py:67
  104.8 4.0 %collective-permute-done.16 = f16[72,512]{1,0:T(8,128)(2,1)S(1)} collective-permute-done((f16[72,512]{1,0:T(8,128)(2,1)S(1)}, f16[72,512]{1,0:T(8,128)(2,1)S(1)}, u32[]{:S(2)}, u32[]{:S(2)}) %collective-permute-start.16) | collective-permute-done | bytes 73760 | tf_op jit(solution)/shard_map/ppermute | solution.py:67
  111.7 3.8 %all-to-all-start = ((f32[32,1,128]{2,1,0:T(1,128)}), f32[32,1,128]{2,1,0:T(1,128)S(1)}, u32[]{:S(2)}, u32[]{:S(2)}) async-start(f32[32,1,128]{2,1,0:T(1,128)} %broadcast_in_dim.23), calls=%async_computation | async-start | bytes 32768 | tf_op jit(solution)/shard_map/all_to_all | solution.py:367
  121.2 2.4 %pad_maximum_fusion = bf16[4,4096,128]{2,1,0:T(8,128)(2,1)S(1)} fusion(bf16[1,4096,128]{2,1,0:T(8,128)(2,1)} %bitcast.12, bf16[1,4096,128]{2,1,0:T(8,128)(2,1)} %bitcast.11, bf16[1,4096,128]{2,1,0:T(8,128)(2,1)} %bitcast.10, bf16[1,4096,128]{2,1,0:T(8,128)(2,1)} %bitcast.153), kind=kLoop, calls=%fused_computation.2 | loop fusion | flops 6291456 | bytes 8388608 | tf_op jit(solution)/shard_map/stack | solution.py:370
  127.8 3.7 %collective-permute-start.17 = (f16[2,32,512]{2,1,0:T(8,128)(2,1)S(1)}, f16[2,32,512]{2,1,0:T(8,128)(2,1)S(1)}, u32[]{:S(2)}, u32[]{:S(2)}) collective-permute-start(f16[2,32,512]{2,1,0:T(8,128)(2,1)S(1)} %fusion.27), channel_id=1, source_target_pairs={{0,24},{4,28},{8,0},{12,4},{16,8},{20,12},{24,16},{28,20},{1,25},{... | collective-permute-start | bytes 196616 | tf_op jit(solution)/shard_map/ppermute | solution.py:67
  132.6 2.4 %slice_bitcast_fusion.1 = (bf16[4096,128]{1,0:T(8,128)(2,1)S(1)}, bf16[4096,128]{1,0:T(8,128)(2,1)S(1)}, bf16[4096,128]{1,0:T(8,128)(2,1)S(1)}, bf16[4096,128]{1,0:T(8,128)(2,1)S(1)}) fusion(bf16[4,4096,128]{2,1,0:T(8,128)(2,1)} %pad_maximum_fusion.1), kind=kLoop, calls=%fused_computation.11 | loop fusion | bytes 8388608 | tf_op jit(solution)/shard_map/squeeze | solution.py:395
  135.4 8.6 %collective-permute-done.17 = f16[2,32,512]{2,1,0:T(8,128)(2,1)S(1)} collective-permute-done((f16[2,32,512]{2,1,0:T(8,128)(2,1)S(1)}, f16[2,32,512]{2,1,0:T(8,128)(2,1)S(1)}, u32[]{:S(2)}, u32[]{:S(2)}) %collective-permute-start.17) | collective-permute-done | bytes 65568 | tf_op jit(solution)/shard_map/ppermute | solution.py:67
  144.0 4.9 %collective-permute-done.18 = f16[2,32,512]{2,1,0:T(8,128)(2,1)S(1)} collective-permute-done((f16[2,32,512]{2,1,0:T(8,128)(2,1)S(1)}, f16[2,32,512]{2,1,0:T(8,128)(2,1)S(1)}, u32[]{:S(2)}, u32[]{:S(2)}) %collective-permute-start.18) | collective-permute-done | bytes 65568 | tf_op jit(solution)/shard_map/ppermute | solution.py:67
  150.2 5.4 %collective-permute-done.20 = f16[4,2,32,512]{3,2,1,0:T(8,128)(2,1)S(1)} collective-permute-done((f16[4,2,32,512]{3,2,1,0:T(8,128)(2,1)S(1)}, f16[4,2,32,512]{3,2,1,0:T(8,128)(2,1)S(1)}, u32[]{:S(2)}, u32[]{:S(2)}) %collective-permute-start.20) | collective-permute-done | bytes 262176 | tf_op jit(solution)/shard_map/ppermute | solution.py:72
  162.5 4.2 %add_convert_fusion = bf16[512,4096]{1,0:T(8,128)(2,1)S(1)} fusion(f16[512,4096]{1,0:T(8,128)(2,1)} %get-tuple-element.72, bf16[256,512]{1,0:T(8,128)(2,1)S(1)} %get-tuple-element.87, bf16[256,512]{1,0:T(8,128)(2,1)S(1)} %get-tuple-element.86, bf16[4096,128]{1,0:T(8,128)(2,1)S(1)} %get-tuple-element.65, bf16[4096,128]{1,0:T(8,128)(2,1)S(1)} %get-tuple-element.64), kind=kOutput, calls=%fused_computation | convolution fusion | flops 2173698048 | bytes 11010048 | tf_op jit(solution)/shard_map/dot_general | solution.py:62
  169.1 4.2 %add_convert_fusion.1 = bf16[4096,512]{1,0:T(8,128)(2,1)S(1)} fusion(f16[4096,512]{1,0:T(8,128)(2,1)} %get-tuple-element.73, bf16[256,512]{1,0:T(8,128)(2,1)S(1)} %get-tuple-element.89, bf16[256,512]{1,0:T(8,128)(2,1)S(1)} %get-tuple-element.88, bf16[4096,128]{1,0:T(8,128)(2,1)S(1)} %get-tuple-element.66, bf16[4096,128]{1,0:T(8,128)(2,1)S(1)} %get-tuple-element.67), kind=kOutput, calls=%fused_computation.1 | convolution fusion | flops 2173698048 | bytes 11010048 | tf_op jit(solution)/shard_map/dot_general | solution.py:62
  173.4 4.8 %collective-permute-done.28 = f16[512,512]{1,0:T(8,128)(2,1)S(1)} collective-permute-done((f16[512,512]{1,0:T(8,128)(2,1)S(1)}, f16[512,512]{1,0:T(8,128)(2,1)S(1)}, u32[]{:S(2)}, u32[]{:S(2)}) %collective-permute-start.28) | collective-permute-done | bytes 524320 | tf_op jit(solution)/shard_map/ppermute | solution.py:280
  (168 shorter events, 68.4 us)
Async XLA Ops:
  1.7 9.6 %collective-permute-start = (bf16[512,128]{1,0:T(8,128)(2,1)S(1)}, bf16[512,128]{1,0:T(8,128)(2,1)S(1)}, u32[]{:S(2)}, u32[]{:S(2)}) collective-permute-start(bf16[512,128]{1,0:T(8,128)(2,1)S(1)} %dynamic-slice_select_fusion.refs_0_), channel_id=1, source_target_pairs={{0,8},{4,12},{8,16},{12,20},{16,24},{20,28},{24,0},{28,4},{1,9},{5... | collective-permute-start | bytes 393224 | tf_op jit(solution)/shard_map/ppermute | solution.py:67
  4.8 11.2 %collective-permute-start.1 = (bf16[512,128]{1,0:T(8,128)(2,1)S(1)}, bf16[512,128]{1,0:T(8,128)(2,1)S(1)}, u32[]{:S(2)}, u32[]{:S(2)}) collective-permute-start(bf16[512,128]{1,0:T(8,128)(2,1)S(1)} %dynamic-slice_select_fusion.refs_0_), channel_id=1, source_target_pairs={{0,16},{4,20},{8,24},{12,28},{16,0},{20,4},{24,8},{28,12},{1,17},{... | collective-permute-start | bytes 393224 | tf_op jit(solution)/shard_map/ppermute | solution.py:67
  7.4 10.2 %collective-permute-start.2 = (bf16[512,128]{1,0:T(8,128)(2,1)S(1)}, bf16[512,128]{1,0:T(8,128)(2,1)S(1)}, u32[]{:S(2)}, u32[]{:S(2)}) collective-permute-start(bf16[512,128]{1,0:T(8,128)(2,1)S(1)} %dynamic-slice_select_fusion.refs_0_), channel_id=1, source_target_pairs={{0,24},{4,28},{8,0},{12,4},{16,8},{20,12},{24,16},{28,20},{1,25},{... | collective-permute-start | bytes 393224 | tf_op jit(solution)/shard_map/ppermute | solution.py:67
  8.7 10.0 %collective-permute-start.3 = (bf16[512,128]{1,0:T(8,128)(2,1)S(1)}, bf16[512,128]{1,0:T(8,128)(2,1)S(1)}, u32[]{:S(2)}, u32[]{:S(2)}) collective-permute-start(bf16[512,128]{1,0:T(8,128)(2,1)S(1)} %dynamic-slice_select_fusion.refs_0_), channel_id=1, source_target_pairs={{0,4},{4,0},{8,12},{12,8},{16,20},{20,16},{24,28},{28,24},{1,5},{5... | collective-permute-start | bytes 393224 | tf_op jit(solution)/shard_map/ppermute | solution.py:72
  30.7 10.4 %collective-permute-start.11 = (f32[768,128]{1,0:T(8,128)}, f32[768,128]{1,0:T(8,128)S(1)}, u32[]{:S(2)}, u32[]{:S(2)}) collective-permute-start(f32[768,128]{1,0:T(8,128)} %get-tuple-element.36.refs_0_), channel_id=1, source_target_pairs={{0,2},{1,3},{2,0},{3,1},{4,6},{5,7},{6,4},{7,5},{8,10},{9,11},{10,... | collective-permute-start | bytes 1179656 | tf_op jit(solution)/shard_map/ppermute | solution.py:72
  32.2 18.8 %collective-permute-start.10 = (f32[768,128]{1,0:T(8,128)}, f32[768,128]{1,0:T(8,128)S(1)}, u32[]{:S(2)}, u32[]{:S(2)}) collective-permute-start(f32[768,128]{1,0:T(8,128)} %get-tuple-element.36.refs_0_), channel_id=1, source_target_pairs={{0,1},{1,0},{2,3},{3,2},{4,5},{5,4},{6,7},{7,6},{8,9},{9,8},{10,11... | collective-permute-start | bytes 1179656 | tf_op jit(solution)/shard_map/ppermute | solution.py:72
  41.0 10.0 %collective-permute-start.12 = (f32[768,128]{1,0:T(8,128)S(1)}, f32[768,128]{1,0:T(8,128)}, u32[]{:S(2)}, u32[]{:S(2)}) collective-permute-start(f32[768,128]{1,0:T(8,128)S(1)} %collective-permute-done.11.refs_2_), channel_id=1, source_target_pairs={{0,1},{1,0},{2,3},{3,2},{4,5},{5,4},{6,7},{7,6},{8,9},{9,8},{10,11... | collective-permute-start | bytes 1179656 | tf_op jit(solution)/shard_map/ppermute | solution.py:72
  44.2 26.3 %collective-permute-start.21 = (f16[2,512,512]{2,1,0:T(8,128)(2,1)}, f16[2,512,512]{2,1,0:T(8,128)(2,1)}, u32[]{:S(2)}, u32[]{:S(2)}) collective-permute-start(f16[2,512,512]{2,1,0:T(8,128)(2,1)} %pad_maximum_fusion.4), channel_id=1, source_target_pairs={{0,8},{8,16},{16,24},{24,28},{28,20},{20,12},{12,4},{4,0},{1,9},{9... | collective-permute-start | bytes 3145736 | tf_op jit(solution)/shard_map/ppermute | solution.py:276
  45.8 25.7 %collective-permute-start.25 = (f16[2,512,512]{2,1,0:T(8,128)(2,1)}, f16[2,512,512]{2,1,0:T(8,128)(2,1)}, u32[]{:S(2)}, u32[]{:S(2)}) collective-permute-start(f16[2,512,512]{2,1,0:T(8,128)(2,1)} %pad_maximum_fusion.4), channel_id=1, source_target_pairs={{8,0},{16,8},{24,16},{28,24},{20,28},{12,20},{4,12},{0,4},{9,1},{1... | collective-permute-start | bytes 3145736 | tf_op jit(solution)/shard_map/ppermute | solution.py:277
  49.5 33.4 %collective-permute-start.8 = (bf16[4096,128]{1,0:T(8,128)(2,1)}, bf16[4096,128]{1,0:T(8,128)(2,1)}, u32[]{:S(2)}, u32[]{:S(2)}) collective-permute-start(bf16[4096,128]{1,0:T(8,128)(2,1)} %get-tuple-element.35), channel_id=1, source_target_pairs={{0,2},{1,3},{2,0},{3,1},{4,6},{5,7},{6,4},{7,5},{8,10},{9,11},{10,... | collective-permute-start | bytes 3145736 | tf_op jit(solution)/shard_map/ppermute | solution.py:72
  51.0 70.2 %collective-permute-start.7 = (bf16[4096,128]{1,0:T(8,128)(2,1)}, bf16[4096,128]{1,0:T(8,128)(2,1)}, u32[]{:S(2)}, u32[]{:S(2)}) collective-permute-start(bf16[4096,128]{1,0:T(8,128)(2,1)} %get-tuple-element.35), channel_id=1, source_target_pairs={{0,1},{1,0},{2,3},{3,2},{4,5},{5,4},{6,7},{7,6},{8,9},{9,8},{10,11... | collective-permute-start | bytes 3145736 | tf_op jit(solution)/shard_map/ppermute | solution.py:72
  57.7 18.5 %collective-permute-start.13 = (f16[264,512]{1,0:T(8,128)(2,1)S(1)}, f16[264,512]{1,0:T(8,128)(2,1)S(1)}, u32[]{:S(2)}, u32[]{:S(2)}) collective-permute-start(f16[264,512]{1,0:T(8,128)(2,1)S(1)} %pad_maximum_fusion.7), channel_id=1, source_target_pairs={{0,4},{4,0},{8,12},{12,8},{16,20},{20,16},{24,28},{28,24},{1,5},{5... | collective-permute-start | bytes 811016 | tf_op jit(solution)/shard_map/ppermute | solution.py:72
  70.5 45.0 %collective-permute-start.22 = (f16[2,512,512]{2,1,0:T(8,128)(2,1)}, f16[2,512,512]{2,1,0:T(8,128)(2,1)}, u32[]{:S(2)}, u32[]{:S(2)}) collective-permute-start(f16[2,512,512]{2,1,0:T(8,128)(2,1)} %collective-permute-done.21), channel_id=1, source_target_pairs={{0,8},{8,16},{16,24},{24,28},{28,20},{20,12},{12,4},{4,0},{1,9},{9... | collective-permute-start | bytes 3145736 | tf_op jit(solution)/shard_map/ppermute | solution.py:276
  71.6 45.9 %collective-permute-start.26 = (f16[2,512,512]{2,1,0:T(8,128)(2,1)}, f16[2,512,512]{2,1,0:T(8,128)(2,1)S(1)}, u32[]{:S(2)}, u32[]{:S(2)}) collective-permute-start(f16[2,512,512]{2,1,0:T(8,128)(2,1)} %collective-permute-done.25), channel_id=1, source_target_pairs={{8,0},{16,8},{24,16},{28,24},{20,28},{12,20},{4,12},{0,4},{9,1},{1... | collective-permute-start | bytes 3145736 | tf_op jit(solution)/shard_map/ppermute | solution.py:277
  80.4 18.1 %collective-permute-start.14 = (f16[72,512]{1,0:T(8,128)(2,1)S(1)}, f16[72,512]{1,0:T(8,128)(2,1)S(1)}, u32[]{:S(2)}, u32[]{:S(2)}) collective-permute-start(f16[72,512]{1,0:T(8,128)(2,1)S(1)} %get-tuple-element.97), channel_id=1, source_target_pairs={{0,8},{4,12},{8,16},{12,20},{16,24},{20,28},{24,0},{28,4},{1,9},{5... | collective-permute-start | bytes 221192 | tf_op jit(solution)/shard_map/ppermute | solution.py:67
  82.8 38.4 %collective-permute-start.9 = (bf16[4096,128]{1,0:T(8,128)(2,1)}, bf16[4096,128]{1,0:T(8,128)(2,1)}, u32[]{:S(2)}, u32[]{:S(2)}) collective-permute-start(bf16[4096,128]{1,0:T(8,128)(2,1)} %collective-permute-done.8), channel_id=1, source_target_pairs={{0,1},{1,0},{2,3},{3,2},{4,5},{5,4},{6,7},{7,6},{8,9},{9,8},{10,11... | collective-permute-start | bytes 3145736 | tf_op jit(solution)/shard_map/ppermute | solution.py:72
  111.7 14.6 %all-to-all-start = ((f32[32,1,128]{2,1,0:T(1,128)}), f32[32,1,128]{2,1,0:T(1,128)S(1)}, u32[]{:S(2)}, u32[]{:S(2)}) async-start(f32[32,1,128]{2,1,0:T(1,128)} %broadcast_in_dim.23), calls=%async_computation | async-start | bytes 32768 | tf_op jit(solution)/shard_map/all_to_all | solution.py:367
  115.6 44.6 %collective-permute-start.23 = (f16[2,512,512]{2,1,0:T(8,128)(2,1)}, f16[2,512,512]{2,1,0:T(8,128)(2,1)S(1)}, u32[]{:S(2)}, u32[]{:S(2)}) collective-permute-start(f16[2,512,512]{2,1,0:T(8,128)(2,1)} %collective-permute-done.22), channel_id=1, source_target_pairs={{0,8},{8,16},{16,24},{24,28},{28,20},{20,12},{12,4},{4,0},{1,9},{9... | collective-permute-start | bytes 3145736 | tf_op jit(solution)/shard_map/ppermute | solution.py:276
  117.4 43.9 %collective-permute-start.27 = (f16[2,512,512]{2,1,0:T(8,128)(2,1)S(1)}, f16[2,512,512]{2,1,0:T(8,128)(2,1)S(1)}, u32[]{:S(2)}, u32[]{:S(2)}) collective-permute-start(f16[2,512,512]{2,1,0:T(8,128)(2,1)S(1)} %collective-permute-done.26), channel_id=1, source_target_pairs={{8,0},{16,8},{24,16},{28,24},{20,28},{12,20},{4,12},{0,4},{9,1},{1... | collective-permute-start | bytes 3145736 | tf_op jit(solution)/shard_map/ppermute | solution.py:277
  127.8 16.2 %collective-permute-start.17 = (f16[2,32,512]{2,1,0:T(8,128)(2,1)S(1)}, f16[2,32,512]{2,1,0:T(8,128)(2,1)S(1)}, u32[]{:S(2)}, u32[]{:S(2)}) collective-permute-start(f16[2,32,512]{2,1,0:T(8,128)(2,1)S(1)} %fusion.27), channel_id=1, source_target_pairs={{0,24},{4,28},{8,0},{12,4},{16,8},{20,12},{24,16},{28,20},{1,25},{... | collective-permute-start | bytes 196616 | tf_op jit(solution)/shard_map/ppermute | solution.py:67
  131.5 17.4 %collective-permute-start.18 = (f16[2,32,512]{2,1,0:T(8,128)(2,1)S(1)}, f16[2,32,512]{2,1,0:T(8,128)(2,1)S(1)}, u32[]{:S(2)}, u32[]{:S(2)}) collective-permute-start(f16[2,32,512]{2,1,0:T(8,128)(2,1)S(1)} %fusion.27), channel_id=1, source_target_pairs={{0,16},{4,20},{8,24},{12,28},{16,0},{20,4},{24,8},{28,12},{1,17},{... | collective-permute-start | bytes 196616 | tf_op jit(solution)/shard_map/ppermute | solution.py:67
  131.5 17.4 %collective-permute-start.19 = (f16[2,32,512]{2,1,0:T(8,128)(2,1)S(1)}, f16[2,32,512]{2,1,0:T(8,128)(2,1)S(1)}, u32[]{:S(2)}, u32[]{:S(2)}) collective-permute-start(f16[2,32,512]{2,1,0:T(8,128)(2,1)S(1)} %fusion.27), channel_id=1, source_target_pairs={{0,8},{4,12},{8,16},{12,20},{16,24},{20,28},{24,0},{28,4},{1,9},{5... | collective-permute-start | bytes 196616 | tf_op jit(solution)/shard_map/ppermute | solution.py:67
  166.9 11.2 %collective-permute-start.28 = (f16[512,512]{1,0:T(8,128)(2,1)S(1)}, f16[512,512]{1,0:T(8,128)(2,1)S(1)}, u32[]{:S(2)}, u32[]{:S(2)}) collective-permute-start(f16[512,512]{1,0:T(8,128)(2,1)S(1)} %slice_bitcast_fusion.9), channel_id=1, source_target_pairs={{8,0},{16,8},{24,16},{28,24},{20,28},{12,20},{4,12},{0,4},{9,1},{1... | collective-permute-start | bytes 1572872 | tf_op jit(solution)/shard_map/ppermute | solution.py:280
  168.0 11.3 %collective-permute-start.24 = (f16[512,512]{1,0:T(8,128)(2,1)S(1)}, f16[512,512]{1,0:T(8,128)(2,1)S(1)}, u32[]{:S(2)}, u32[]{:S(2)}) collective-permute-start(f16[512,512]{1,0:T(8,128)(2,1)S(1)} %slice_bitcast_fusion.15), channel_id=1, source_target_pairs={{0,8},{8,16},{16,24},{24,28},{28,20},{20,12},{12,4},{4,0},{1,9},{9... | collective-permute-start | bytes 1572872 | tf_op jit(solution)/shard_map/ppermute | solution.py:279
  (36 other events, 247.0 us)

commit v2 on v1

--- a/solution.py
+++ b/solution.py
@@ -62,11 +62,6 @@
     return lax.dot_general(a, b, (dims, ((), ())), preferred_element_type=f32)
 
 
-def shift(x, axis, k):
-    n = lax.axis_size(axis)
-    return lax.ppermute(x, axis, [(i, (i + k) % n) for i in range(n)])
-
-
 def swap(x, axis, bit):
     n = lax.axis_size(axis)
     return lax.ppermute(x, axis, [(i, i ^ bit) for i in range(n)])
@@ -81,9 +76,9 @@
     half = n // 2
     me = lax.axis_index("fs")
     outer, inner = me // 2, me % 2
-    line = [x] + [shift(x, "fs", 2 * k) for k in range(1, half)]
+    line = [x] + [swap(x, "fs", 2 * k) for k in range(1, half)]
     across = [swap(block, "fs", 1) for block in line]
-    places = [(outer - k) % half * 2 for k in range(half)]
+    places = [(outer ^ k) * 2 for k in range(half)]
     return line + across, [p + inner for p in places] + [p + 1 - inner for p in places]
 
 
@@ -103,9 +98,13 @@
     half = n // 2
     me = lax.axis_index("fs")
     outer, inner = me // 2, me % 2
-    arrived = [x[None]] + [shift(x, "fs", 2 * k)[None] for k in range(1, half)]
-    turned = arrived[:0:-1] + arrived[:1] + arrived[:0:-1]
-    mine = lax.dynamic_slice_in_dim(jnp.concatenate(turned, axis=0), half - 1 - outer, half, 0)
+    arrived = [x] + [swap(x, "fs", 2 * k) for k in range(1, half)]
+    mine = jnp.stack(arrived)
+    bit = half // 2
+    while bit:
+        pairs = mine.reshape((half // (2 * bit), 2, bit) + x.shape)
+        mine = jnp.where((outer // bit) % 2 == 0, pairs, pairs[:, ::-1]).reshape(mine.shape)
+        bit //= 2
     other = swap(mine, "fs", 1)
     lower = jnp.where(inner == 0, mine, other)
     upper = jnp.where(inner == 0, other, mine)
@@ -155,6 +154,7 @@
         out_specs=(VMEM, VMEM),
         scratch_shapes=[pltpu.VMEM((count, width), bf16), pltpu.SemaphoreType.DMA((parts,))],
         cost_estimate=pl.CostEstimate(flops=2 * count * width * 256, bytes_accessed=2 * count * width, transcendentals=0),
+        compiler_params=pltpu.CompilerParams(vmem_limit_bytes=56 * 2**20),
         name="map_tokens",
     )(at, *blocks, *tokens)
 
@@ -185,15 +185,17 @@
             tall = jnp.abs(total[m])
             top = jnp.maximum(top, jnp.max(tall.reshape(rank // 8, 8, cols), axis=0))
         peak[...] = jnp.max(top, axis=(0, 1), keepdims=True) + jnp.zeros((8, cols), f32)
-        for o in range(n // 2):
+        for k in range(n // 2):
+            o = at[t + 1] ^ k
             for m in range(2):
                 first = pl.multiple_of((2 * o + at[t]) * rows, rows)
-                keep[o, m] = total[m, pl.ds(first, rows), :]
+                keep[k, m] = total[m, pl.ds(first, rows), :]
                 other = pl.multiple_of((2 * o + 1 - at[t]) * rows, rows)
-                send[o, m] = total[m, pl.ds(other, rows), :]
+                send[k, m] = total[m, pl.ds(other, rows), :]
 
     me = lax.axis_index("tp")
-    at = jnp.stack([me ^ r for r in range(t)] + [lax.axis_index("fs") % 2]).astype(jnp.int32)
+    here = lax.axis_index("fs")
+    at = jnp.stack([me ^ r for r in range(t)] + [here % 2, here // 2]).astype(jnp.int32)
     shape = jax.ShapeDtypeStruct((n // 2, 2, rows, cols), f32)
     return pl.pallas_call(
         kernel,
@@ -202,6 +204,7 @@
         out_specs=(VMEM, VMEM, VMEM),
         scratch_shapes=[pltpu.VMEM((2, count, cols), bf16), pltpu.VMEM((2, rank, cols), f32)],
         cost_estimate=pl.CostEstimate(flops=8 * count * rank * cols, bytes_accessed=4 * rank * cols, transcendentals=0),
+        compiler_params=pltpu.CompilerParams(vmem_limit_bytes=14 * 2**20),
         name="low_rank",
     )(at, *mapped, *rights)
 
@@ -218,26 +221,6 @@
 def unpack(packed, shape):
     power = packed[-8:].astype(f32)
     return (packed[:-8].astype(f32) * jnp.exp2(-power[:1])).reshape(shape), power
-
-
-def add_blocks(keep, came):
-    half = keep.shape[0]
-
-    def kernel(at, a, b, *outs):
-        for k in range(half):
-            o = (at[0] + k) % half
-            outs[k][...] = a[o] + b[o]
-
-    at = jnp.stack([lax.axis_index("fs") // 2]).astype(jnp.int32)
-    shape = jax.ShapeDtypeStruct(keep.shape[1:], f32)
-    return pl.pallas_call(
-        kernel,
-        out_shape=(shape,) * half,
-        in_specs=[SMEM, VMEM, VMEM],
-        out_specs=(VMEM,) * half,
-        cost_estimate=pl.CostEstimate(flops=keep.size, bytes_accessed=8 * keep.size, transcendentals=0),
-        name="add_blocks",
-    )(at, keep, came)
 
 
 def ring_tables():
@@ -299,9 +282,11 @@
 
     def whole(self, value, output):
         rows, cols = self.shapes[0][0], self.shapes[1][1]
-        for index, v, o in self.blocks[1:-1]:
-            value = put(value, v, index * rows, 0)
-            output = put(output, o, index * cols, 1)
+        steps = list(range(1, self.steps))
+        for s in steps[1:2] + steps[:1] + steps[2:]:
+            for index, v, o in self.blocks[2 * s - 1 : 2 * s + 1]:
+                value = put(value, v, index * rows, 0)
+                output = put(output, o, index * cols, 1)
         return value, output
 
 
@@ -357,9 +342,9 @@
     came, power = unpack(packed, send.shape)
     power = scale_of(peak + jnp.exp2(15.0 - power))
     pieces = blocks_tp(piece)
-    sums = add_blocks(keep, came)
+    sums = keep + came
     packed = [pack(sums[k], power) for k in range(1, n // 2)]
-    packed = [shift(p, "fs", 2 * (k + 1)) for k, p in enumerate(packed)]
+    packed = [swap(p, "fs", 2 * (k + 1)) for k, p in enumerate(packed)]
     low = sums[0]
     for p in packed:
         low = low + unpack(p, low.shape)[0]

time: 184 us -> 179 us (0.973)
  waiting for transfers between devices: 74.8 us -> 87 us
  other arithmetic: 16.7 us -> 10.6 us
  Pallas kernels: 13.5 us -> 9.21 us
  local copies, waits for them, and re-layouts: 29.4 us -> 25.9 us
  matrix products: 12.3 us -> 9.28 us
    ppermute x12 -> x21, waiting for transfers between devices: 20.9 us -> 65 us  [swap(): return lax.ppermute(x, axis, [(i, i ^ bit) for i in range(n)])]
    ppermute x9 -> x0, waiting for transfers between devices: 43.2 us -> none  [shift(): return lax.ppermute(x, axis, [(i, (i + k) % n) for i in range(n)])]
    ppermute x9 -> x0, starting transfers between devices: 12.1 us -> none  [shift(): return lax.ppermute(x, axis, [(i, (i + k) % n) for i in range(n)])]
    ppermute x12 -> x21, starting transfers between devices: 10.7 us -> 21.5 us  [swap(): return lax.ppermute(x, axis, [(i, i ^ bit) for i in range(n)])]
    ppermute x3, waiting for transfers between devices: 4.68 us -> 14.2 us  [send(): self.down = lax.ppermute(self.down, 'fs', self.ahead)]
    unnamed x65 -> x74, local copies, waits for them, and re-layouts: 6.34 us -> 9.93 us
    dot_general x6, matrix products: 12.3 us -> 9.28 us  [dot(): return lax.dot_general(a, b, (dims, ((), ())), preferred_element_type=f32)]
    ppermute x3, starting transfers between devices: 4.44 us -> 7.25 us  [send(): self.down = lax.ppermute(self.down, 'fs', self.ahead)]
  transfers between devices with their start and end apart: 30 -> 30, of which waited for: 15 -> 16; matrix products, arithmetic and copies ran while one was open for 25% -> 18% of each run, Pallas kernels for 4% -> 2%
where the time goes in v2:
time: 179 us
  waiting for transfers between devices  87 us (49%)
  starting transfers between devices  34.6 us (19%)
  local copies, waits for them, and re-layouts  25.9 us (14%)
  other arithmetic  10.6 us (6%)
  matrix products  9.28 us (5%)
  Pallas kernels  9.21 us (5%)
  between operations  2.15 us (1%)
    ppermute x21, waiting for transfers between devices, swap(): return lax.ppermute(x, axis, [(i, i ^ bit) for i in range(n)])  65 us
    ppermute x21, starting transfers between devices, swap(): return lax.ppermute(x, axis, [(i, i ^ bit) for i in range(n)])  21.5 us
    ppermute x3, waiting for transfers between devices, send(): self.down = lax.ppermute(self.down, 'fs', self.ahead)  14.2 us
    dynamic_update_slice x8, local copies, waits for them, and re-layouts, put(): return lax.dynamic_update_slice_in_dim(whole, block, index, dim)  10.3 us
    unnamed x74, local copies, waits for them, and re-layouts  9.93 us
    dot_general x6, matrix products, dot(): return lax.dot_general(a, b, (dims, ((), ())), preferred_element_type=f32)  9.28 us
    ppermute x3, starting transfers between devices, send(): self.down = lax.ppermute(self.down, 'fs', self.ahead)  7.25 us
    ppermute x1, waiting for transfers between devices, send(): self.up = lax.ppermute(self.up[1], 'fs', self.back)  6.71 us
  transfers between devices with their start and end apart: 30, of which 16 were waited for; matrix products, arithmetic and copies ran while one was open for 18% of the time, Pallas kernels for 2%

profile of v2, /device:TPU:0, one launch (start us, length us, event | category | flops | bytes accessed | tf_op | source)
XLA Modules:
  0.0 178.8 jit_solution(2187610227646595297)
XLA Ops:
  1.7 3.1 %collective-permute-start = (bf16[512,128]{1,0:T(8,128)(2,1)S(1)}, bf16[512,128]{1,0:T(8,128)(2,1)S(1)}, u32[]{:S(2)}, u32[]{:S(2)}) collective-permute-start(bf16[512,128]{1,0:T(8,128)(2,1)S(1)} %dynamic-slice_select_fusion.refs_0_), channel_id=1, source_target_pairs={{0,8},{4,12},{8,0},{12,4},{16,24},{20,28},{24,16},{28,20},{1,9},{5... | collective-permute-start | bytes 393224 | tf_op jit(solution)/shard_map/ppermute | solution.py:67
  4.8 2.6 %collective-permute-start.1 = (bf16[512,128]{1,0:T(8,128)(2,1)S(1)}, bf16[512,128]{1,0:T(8,128)(2,1)S(1)}, u32[]{:S(2)}, u32[]{:S(2)}) collective-permute-start(bf16[512,128]{1,0:T(8,128)(2,1)S(1)} %dynamic-slice_select_fusion.refs_0_), channel_id=1, source_target_pairs={{0,16},{4,20},{8,24},{12,28},{16,0},{20,4},{24,8},{28,12},{1,17},{... | collective-permute-start | bytes 393224 | tf_op jit(solution)/shard_map/ppermute | solution.py:67
  11.6 6.1 %collective-permute-done.1.refs_2_ = bf16[512,128]{1,0:T(8,128)(2,1)S(1)} collective-permute-done((bf16[512,128]{1,0:T(8,128)(2,1)S(1)}, bf16[512,128]{1,0:T(8,128)(2,1)S(1)}, u32[]{:S(2)}, u32[]{:S(2)}) %collective-permute-start.1) | collective-permute-done | bytes 131104 | tf_op jit(solution)/shard_map/ppermute | solution.py:67
  24.9 5.7 %map_tokens.1 = (f32[768,128]{1,0:T(8,128)}, bf16[4096,128]{1,0:T(8,128)(2,1)}) custom-call(s32[9]{0:T(128)} %stack.124.at, bf16[512,128]{1,0:T(8,128)(2,1)} %copy-done.19, bf16[512,128]{1,0:T(8,128)(2,1)} %copy-done.24, bf16[512,128]{1,0:T(8,128)(2,1)} %copy-done.25, bf16[512,128]{1,0:T(8,128)(2,1)} %copy-done.26, bf16[512,128]{1,0:T(8,128)(2,1)} %copy-done.27, ...), custom_call_target="tpu_custom_call" | custom-call | flops 1610612736 | bytes 6291456 | tf_op jit(solution)/shard_map/map_tokens/pallas_call | solution.py:147
  32.2 6.5 %collective-permute-done.11.refs_2_ = f32[768,128]{1,0:T(8,128)S(1)} collective-permute-done((f32[768,128]{1,0:T(8,128)}, f32[768,128]{1,0:T(8,128)S(1)}, u32[]{:S(2)}, u32[]{:S(2)}) %collective-permute-start.11) | collective-permute-done | bytes 393248 | tf_op jit(solution)/shard_map/ppermute | solution.py:67
  40.3 2.9 %collective-permute-start.21 = (f16[2,512,512]{2,1,0:T(8,128)(2,1)}, f16[2,512,512]{2,1,0:T(8,128)(2,1)}, u32[]{:S(2)}, u32[]{:S(2)}) collective-permute-start(f16[2,512,512]{2,1,0:T(8,128)(2,1)} %pad_maximum_fusion.4), channel_id=1, source_target_pairs={{0,8},{8,16},{16,24},{24,28},{28,20},{20,12},{12,4},{4,0},{1,9},{9... | collective-permute-start | bytes 3145736 | tf_op jit(solution)/shard_map/ppermute | solution.py:259
  52.4 14.2 %collective-permute-done.21 = f16[2,512,512]{2,1,0:T(8,128)(2,1)} collective-permute-done((f16[2,512,512]{2,1,0:T(8,128)(2,1)}, f16[2,512,512]{2,1,0:T(8,128)(2,1)}, u32[]{:S(2)}, u32[]{:S(2)}) %collective-permute-start.21) | collective-permute-done | bytes 1048608 | tf_op jit(solution)/shard_map/ppermute | solution.py:259
  66.6 2.5 %collective-permute-start.22 = (f16[2,512,512]{2,1,0:T(8,128)(2,1)}, f16[2,512,512]{2,1,0:T(8,128)(2,1)}, u32[]{:S(2)}, u32[]{:S(2)}) collective-permute-start(f16[2,512,512]{2,1,0:T(8,128)(2,1)} %collective-permute-done.21), channel_id=1, source_target_pairs={{0,8},{8,16},{16,24},{24,28},{28,20},{20,12},{12,4},{4,0},{1,9},{9... | collective-permute-start | bytes 3145736 | tf_op jit(solution)/shard_map/ppermute | solution.py:259
  70.3 2.5 %collective-permute-done.13 = f16[264,512]{1,0:T(8,128)(2,1)S(1)} collective-permute-done((f16[264,512]{1,0:T(8,128)(2,1)S(1)}, f16[264,512]{1,0:T(8,128)(2,1)S(1)}, u32[]{:S(2)}, u32[]{:S(2)}) %collective-permute-start.13) | collective-permute-done | bytes 270368 | tf_op jit(solution)/shard_map/ppermute | solution.py:67
  76.2 19.1 %collective-permute-done.14 = f16[72,512]{1,0:T(8,128)(2,1)S(1)} collective-permute-done((f16[72,512]{1,0:T(8,128)(2,1)S(1)}, f16[72,512]{1,0:T(8,128)(2,1)S(1)}, u32[]{:S(2)}, u32[]{:S(2)}) %collective-permute-start.14) | collective-permute-done | bytes 73760 | tf_op jit(solution)/shard_map/ppermute | solution.py:67
  95.5 6.0 %collective-permute-done.15 = f16[72,512]{1,0:T(8,128)(2,1)S(1)} collective-permute-done((f16[72,512]{1,0:T(8,128)(2,1)S(1)}, f16[72,512]{1,0:T(8,128)(2,1)S(1)}, u32[]{:S(2)}, u32[]{:S(2)}) %collective-permute-start.15) | collective-permute-done | bytes 73760 | tf_op jit(solution)/shard_map/ppermute | solution.py:67
  101.5 6.1 %collective-permute-done.16 = f16[72,512]{1,0:T(8,128)(2,1)S(1)} collective-permute-done((f16[72,512]{1,0:T(8,128)(2,1)S(1)}, f16[72,512]{1,0:T(8,128)(2,1)S(1)}, u32[]{:S(2)}, u32[]{:S(2)}) %collective-permute-start.16) | collective-permute-done | bytes 73760 | tf_op jit(solution)/shard_map/ppermute | solution.py:67
  109.6 3.0 %all-to-all-start = ((f32[32,1,128]{2,1,0:T(1,128)}), f32[32,1,128]{2,1,0:T(1,128)S(1)}, u32[]{:S(2)}, u32[]{:S(2)}) async-start(f32[32,1,128]{2,1,0:T(1,128)} %broadcast_in_dim.13), calls=%async_computation | async-start | bytes 32768 | tf_op jit(solution)/shard_map/all_to_all | solution.py:352
  114.7 2.4 %fusion.8 = (f16[512,4096]{1,0:T(8,128)(2,1)}, f16[4096,512]{1,0:T(8,128)(2,1)}) fusion(f16[512,4096]{1,0:T(8,128)(2,1)} %copy-done.10, s32[]{:T(128)S(6)} %select_n.233, f16[2,512,512]{2,1,0:T(8,128)(2,1)} %collective-permute-done.22, f16[4096,512]{1,0:T(8,128)(2,1)} %copy-done.8), kind=kLoop, calls=%fused_computation.35 | loop fusion | bytes 2097156 | tf_op jit(solution)/shard_map/dynamic_update_slice | solution.py:71
  117.1 2.4 %fusion.7 = (f16[512,4096]{1,0:T(8,128)(2,1)}, f16[4096,512]{1,0:T(8,128)(2,1)}) fusion(f16[512,4096]{1,0:T(8,128)(2,1)} %get-tuple-element.72, s32[]{:T(128)S(6)} %select_n.236, f16[2,512,512]{2,1,0:T(8,128)(2,1)} %collective-permute-done.26, f16[4096,512]{1,0:T(8,128)(2,1)} %get-tuple-element.73), kind=kLoop, calls=%fused_computation.33 | loop fusion | bytes 2097156 | tf_op jit(solution)/shard_map/dynamic_update_slice | solution.py:71
  119.4 2.4 %fusion.6 = (f16[512,4096]{1,0:T(8,128)(2,1)}, f16[4096,512]{1,0:T(8,128)(2,1)}) fusion(f16[512,4096]{1,0:T(8,128)(2,1)} %get-tuple-element.70, s32[]{:T(128)S(6)} %select_n.239, f16[2,512,512]{2,1,0:T(8,128)(2,1)} %collective-permute-done.21, f16[4096,512]{1,0:T(8,128)(2,1)} %get-tuple-element.71), kind=kLoop, calls=%fused_computation.31 | loop fusion | bytes 2097156 | tf_op jit(solution)/shard_map/dynamic_update_slice | solution.py:71
  121.8 2.4 %fusion.5 = (f16[512,4096]{1,0:T(8,128)(2,1)}, f16[4096,512]{1,0:T(8,128)(2,1)}) fusion(f16[512,4096]{1,0:T(8,128)(2,1)} %get-tuple-element.68, s32[]{:T(128)S(6)} %select_n.242, f16[2,512,512]{2,1,0:T(8,128)(2,1)} %collective-permute-done.25, f16[4096,512]{1,0:T(8,128)(2,1)} %get-tuple-element.69), kind=kLoop, calls=%fused_computation.29 | loop fusion | bytes 2097156 | tf_op jit(solution)/shard_map/dynamic_update_slice | solution.py:71
  132.3 2.4 %collective-permute-start.18 = (f16[2,32,512]{2,1,0:T(8,128)(2,1)S(1)}, f16[2,32,512]{2,1,0:T(8,128)(2,1)S(1)}, u32[]{:S(2)}, u32[]{:S(2)}) collective-permute-start(f16[2,32,512]{2,1,0:T(8,128)(2,1)S(1)} %fusion.29), channel_id=1, source_target_pairs={{0,16},{4,20},{8,24},{12,28},{16,0},{20,4},{24,8},{28,12},{1,17},{... | collective-permute-start | bytes 196616 | tf_op jit(solution)/shard_map/ppermute | solution.py:67
  135.0 2.4 %slice_bitcast_fusion.1 = (bf16[4096,128]{1,0:T(8,128)(2,1)S(1)}, bf16[4096,128]{1,0:T(8,128)(2,1)S(1)}, bf16[4096,128]{1,0:T(8,128)(2,1)S(1)}, bf16[4096,128]{1,0:T(8,128)(2,1)S(1)}) fusion(bf16[4,4096,128]{2,1,0:T(8,128)(2,1)} %pad_maximum_fusion.1), kind=kLoop, calls=%fused_computation.11 | loop fusion | bytes 8388608 | tf_op jit(solution)/shard_map/squeeze | solution.py:380
  137.8 4.0 %collective-permute-done.17 = f16[2,32,512]{2,1,0:T(8,128)(2,1)S(1)} collective-permute-done((f16[2,32,512]{2,1,0:T(8,128)(2,1)S(1)}, f16[2,32,512]{2,1,0:T(8,128)(2,1)S(1)}, u32[]{:S(2)}, u32[]{:S(2)}) %collective-permute-start.17) | collective-permute-done | bytes 65568 | tf_op jit(solution)/shard_map/ppermute | solution.py:67
  146.7 6.2 %collective-permute-done.20 = f16[4,2,32,512]{3,2,1,0:T(8,128)(2,1)S(1)} collective-permute-done((f16[4,2,32,512]{3,2,1,0:T(8,128)(2,1)S(1)}, f16[4,2,32,512]{3,2,1,0:T(8,128)(2,1)S(1)}, u32[]{:S(2)}, u32[]{:S(2)}) %collective-permute-start.20) | collective-permute-done | bytes 262176 | tf_op jit(solution)/shard_map/ppermute | solution.py:67
  158.9 2.7 %add_convert_fusion = bf16[512,4096]{1,0:T(8,128)(2,1)S(1)} fusion(f16[512,4096]{1,0:T(8,128)(2,1)S(1)} %get-tuple-element.62, bf16[256,512]{1,0:T(8,128)(2,1)S(1)} %get-tuple-element.77, bf16[256,512]{1,0:T(8,128)(2,1)S(1)} %get-tuple-element.76, bf16[4096,128]{1,0:T(8,128)(2,1)S(1)} %get-tuple-element.55, bf16[4096,128]{1,0:T(8,128)(2,1)S(1)} %get-tuple-element.54), kind=kOutput, calls=%fused_computation | convolution fusion | flops 2173698048 | bytes 11010048 | tf_op jit(solution)/shard_map/dot_general | solution.py:62
  164.0 2.8 %add_convert_fusion.1 = bf16[4096,512]{1,0:T(8,128)(2,1)S(1)} fusion(f16[4096,512]{1,0:T(8,128)(2,1)S(1)} %get-tuple-element.63, bf16[256,512]{1,0:T(8,128)(2,1)S(1)} %get-tuple-element.79, bf16[256,512]{1,0:T(8,128)(2,1)S(1)} %get-tuple-element.78, bf16[4096,128]{1,0:T(8,128)(2,1)S(1)} %get-tuple-element.56, bf16[4096,128]{1,0:T(8,128)(2,1)S(1)} %get-tuple-element.57), kind=kOutput, calls=%fused_computation.1 | convolution fusion | flops 2173698048 | bytes 11010048 | tf_op jit(solution)/shard_map/dot_general | solution.py:62
  166.8 6.7 %collective-permute-done.28 = f16[512,512]{1,0:T(8,128)(2,1)S(1)} collective-permute-done((f16[512,512]{1,0:T(8,128)(2,1)S(1)}, f16[512,512]{1,0:T(8,128)(2,1)S(1)}, u32[]{:S(2)}, u32[]{:S(2)}) %collective-permute-start.28) | collective-permute-done | bytes 524320 | tf_op jit(solution)/shard_map/ppermute | solution.py:263
  (176 shorter events, 59.5 us)
Async XLA Ops:
  1.7 8.2 %collective-permute-start = (bf16[512,128]{1,0:T(8,128)(2,1)S(1)}, bf16[512,128]{1,0:T(8,128)(2,1)S(1)}, u32[]{:S(2)}, u32[]{:S(2)}) collective-permute-start(bf16[512,128]{1,0:T(8,128)(2,1)S(1)} %dynamic-slice_select_fusion.refs_0_), channel_id=1, source_target_pairs={{0,8},{4,12},{8,0},{12,4},{16,24},{20,28},{24,16},{28,20},{1,9},{5... | collective-permute-start | bytes 393224 | tf_op jit(solution)/shard_map/ppermute | solution.py:67
  4.8 12.9 %collective-permute-start.1 = (bf16[512,128]{1,0:T(8,128)(2,1)S(1)}, bf16[512,128]{1,0:T(8,128)(2,1)S(1)}, u32[]{:S(2)}, u32[]{:S(2)}) collective-permute-start(bf16[512,128]{1,0:T(8,128)(2,1)S(1)} %dynamic-slice_select_fusion.refs_0_), channel_id=1, source_target_pairs={{0,16},{4,20},{8,24},{12,28},{16,0},{20,4},{24,8},{28,12},{1,17},{... | collective-permute-start | bytes 393224 | tf_op jit(solution)/shard_map/ppermute | solution.py:67
  7.4 11.8 %collective-permute-start.2 = (bf16[512,128]{1,0:T(8,128)(2,1)S(1)}, bf16[512,128]{1,0:T(8,128)(2,1)S(1)}, u32[]{:S(2)}, u32[]{:S(2)}) collective-permute-start(bf16[512,128]{1,0:T(8,128)(2,1)S(1)} %dynamic-slice_select_fusion.refs_0_), channel_id=1, source_target_pairs={{0,24},{4,28},{8,16},{12,20},{16,8},{20,12},{24,0},{28,4},{1,25},{... | collective-permute-start | bytes 393224 | tf_op jit(solution)/shard_map/ppermute | solution.py:67
  7.4 12.9 %collective-permute-start.3 = (bf16[512,128]{1,0:T(8,128)(2,1)S(1)}, bf16[512,128]{1,0:T(8,128)(2,1)S(1)}, u32[]{:S(2)}, u32[]{:S(2)}) collective-permute-start(bf16[512,128]{1,0:T(8,128)(2,1)S(1)} %dynamic-slice_select_fusion.refs_0_), channel_id=1, source_target_pairs={{0,4},{4,0},{8,12},{12,8},{16,20},{20,16},{24,28},{28,24},{1,5},{5... | collective-permute-start | bytes 393224 | tf_op jit(solution)/shard_map/ppermute | solution.py:67
  9.9 10.5 %collective-permute-start.4 = (bf16[512,128]{1,0:T(8,128)(2,1)S(1)}, bf16[512,128]{1,0:T(8,128)(2,1)S(1)}, u32[]{:S(2)}, u32[]{:S(2)}) collective-permute-start(bf16[512,128]{1,0:T(8,128)(2,1)S(1)} %collective-permute-done.refs_1_), channel_id=1, source_target_pairs={{0,4},{4,0},{8,12},{12,8},{16,20},{20,16},{24,28},{28,24},{1,5},{5... | collective-permute-start | bytes 393224 | tf_op jit(solution)/shard_map/ppermute | solution.py:67
  32.2 15.0 %collective-permute-start.10 = (f32[768,128]{1,0:T(8,128)}, f32[768,128]{1,0:T(8,128)S(1)}, u32[]{:S(2)}, u32[]{:S(2)}) collective-permute-start(f32[768,128]{1,0:T(8,128)} %get-tuple-element.32.refs_0_), channel_id=1, source_target_pairs={{0,1},{1,0},{2,3},{3,2},{4,5},{5,4},{6,7},{7,6},{8,9},{9,8},{10,11... | collective-permute-start | bytes 1179656 | tf_op jit(solution)/shard_map/ppermute | solution.py:67
  38.7 8.6 %collective-permute-start.12 = (f32[768,128]{1,0:T(8,128)S(1)}, f32[768,128]{1,0:T(8,128)S(1)}, u32[]{:S(2)}, u32[]{:S(2)}) collective-permute-start(f32[768,128]{1,0:T(8,128)S(1)} %collective-permute-done.11.refs_2_), channel_id=1, source_target_pairs={{0,1},{1,0},{2,3},{3,2},{4,5},{5,4},{6,7},{7,6},{8,9},{9,8},{10,11... | collective-permute-start | bytes 1179656 | tf_op jit(solution)/shard_map/ppermute | solution.py:67
  40.3 26.3 %collective-permute-start.21 = (f16[2,512,512]{2,1,0:T(8,128)(2,1)}, f16[2,512,512]{2,1,0:T(8,128)(2,1)}, u32[]{:S(2)}, u32[]{:S(2)}) collective-permute-start(f16[2,512,512]{2,1,0:T(8,128)(2,1)} %pad_maximum_fusion.4), channel_id=1, source_target_pairs={{0,8},{8,16},{16,24},{24,28},{28,20},{20,12},{12,4},{4,0},{1,9},{9... | collective-permute-start | bytes 3145736 | tf_op jit(solution)/shard_map/ppermute | solution.py:259
  43.2 25.9 %collective-permute-start.25 = (f16[2,512,512]{2,1,0:T(8,128)(2,1)}, f16[2,512,512]{2,1,0:T(8,128)(2,1)}, u32[]{:S(2)}, u32[]{:S(2)}) collective-permute-start(f16[2,512,512]{2,1,0:T(8,128)(2,1)} %pad_maximum_fusion.4), channel_id=1, source_target_pairs={{8,0},{16,8},{24,16},{28,24},{20,28},{12,20},{4,12},{0,4},{9,1},{1... | collective-permute-start | bytes 3145736 | tf_op jit(solution)/shard_map/ppermute | solution.py:260
  49.3 23.5 %collective-permute-start.13 = (f16[264,512]{1,0:T(8,128)(2,1)S(1)}, f16[264,512]{1,0:T(8,128)(2,1)S(1)}, u32[]{:S(2)}, u32[]{:S(2)}) collective-permute-start(f16[264,512]{1,0:T(8,128)(2,1)S(1)} %pad_maximum_fusion.7), channel_id=1, source_target_pairs={{0,4},{4,0},{8,12},{12,8},{16,20},{20,16},{24,28},{28,24},{1,5},{5... | collective-permute-start | bytes 811016 | tf_op jit(solution)/shard_map/ppermute | solution.py:67
  50.9 25.3 %collective-permute-start.8 = (bf16[4096,128]{1,0:T(8,128)(2,1)}, bf16[4096,128]{1,0:T(8,128)(2,1)}, u32[]{:S(2)}, u32[]{:S(2)}) collective-permute-start(bf16[4096,128]{1,0:T(8,128)(2,1)} %get-tuple-element.31), channel_id=1, source_target_pairs={{0,2},{1,3},{2,0},{3,1},{4,6},{5,7},{6,4},{7,5},{8,10},{9,11},{10,... | collective-permute-start | bytes 3145736 | tf_op jit(solution)/shard_map/ppermute | solution.py:67
  52.4 71.8 %collective-permute-start.7 = (bf16[4096,128]{1,0:T(8,128)(2,1)}, bf16[4096,128]{1,0:T(8,128)(2,1)}, u32[]{:S(2)}, u32[]{:S(2)}) collective-permute-start(bf16[4096,128]{1,0:T(8,128)(2,1)} %get-tuple-element.31), channel_id=1, source_target_pairs={{0,1},{1,0},{2,3},{3,2},{4,5},{5,4},{6,7},{7,6},{8,9},{9,8},{10,11... | collective-permute-start | bytes 3145736 | tf_op jit(solution)/shard_map/ppermute | solution.py:67
  66.6 46.0 %collective-permute-start.22 = (f16[2,512,512]{2,1,0:T(8,128)(2,1)}, f16[2,512,512]{2,1,0:T(8,128)(2,1)}, u32[]{:S(2)}, u32[]{:S(2)}) collective-permute-start(f16[2,512,512]{2,1,0:T(8,128)(2,1)} %collective-permute-done.21), channel_id=1, source_target_pairs={{0,8},{8,16},{16,24},{24,28},{28,20},{20,12},{12,4},{4,0},{1,9},{9... | collective-permute-start | bytes 3145736 | tf_op jit(solution)/shard_map/ppermute | solution.py:259
  69.1 45.3 %collective-permute-start.26 = (f16[2,512,512]{2,1,0:T(8,128)(2,1)}, f16[2,512,512]{2,1,0:T(8,128)(2,1)}, u32[]{:S(2)}, u32[]{:S(2)}) collective-permute-start(f16[2,512,512]{2,1,0:T(8,128)(2,1)} %collective-permute-done.25), channel_id=1, source_target_pairs={{8,0},{16,8},{24,16},{28,24},{20,28},{12,20},{4,12},{0,4},{9,1},{1... | collective-permute-start | bytes 3145736 | tf_op jit(solution)/shard_map/ppermute | solution.py:260
  73.2 22.1 %collective-permute-start.14 = (f16[72,512]{1,0:T(8,128)(2,1)S(1)}, f16[72,512]{1,0:T(8,128)(2,1)S(1)}, u32[]{:S(2)}, u32[]{:S(2)}) collective-permute-start(f16[72,512]{1,0:T(8,128)(2,1)S(1)} %get-tuple-element.95), channel_id=1, source_target_pairs={{0,8},{4,12},{8,0},{12,4},{16,24},{20,28},{24,16},{28,20},{1,9},{5... | collective-permute-start | bytes 221192 | tf_op jit(solution)/shard_map/ppermute | solution.py:67
  76.2 48.0 %collective-permute-start.9 = (bf16[4096,128]{1,0:T(8,128)(2,1)}, bf16[4096,128]{1,0:T(8,128)(2,1)}, u32[]{:S(2)}, u32[]{:S(2)}) collective-permute-start(bf16[4096,128]{1,0:T(8,128)(2,1)} %collective-permute-done.8), channel_id=1, source_target_pairs={{0,1},{1,0},{2,3},{3,2},{4,5},{5,4},{6,7},{7,6},{8,9},{9,8},{10,11... | collective-permute-start | bytes 3145736 | tf_op jit(solution)/shard_map/ppermute | solution.py:67
  109.6 19.4 %all-to-all-start = ((f32[32,1,128]{2,1,0:T(1,128)}), f32[32,1,128]{2,1,0:T(1,128)S(1)}, u32[]{:S(2)}, u32[]{:S(2)}) async-start(f32[32,1,128]{2,1,0:T(1,128)} %broadcast_in_dim.13), calls=%async_computation | async-start | bytes 32768 | tf_op jit(solution)/shard_map/all_to_all | solution.py:352
  112.6 44.8 %collective-permute-start.23 = (f16[2,512,512]{2,1,0:T(8,128)(2,1)}, f16[2,512,512]{2,1,0:T(8,128)(2,1)S(1)}, u32[]{:S(2)}, u32[]{:S(2)}) collective-permute-start(f16[2,512,512]{2,1,0:T(8,128)(2,1)} %collective-permute-done.22), channel_id=1, source_target_pairs={{0,8},{8,16},{16,24},{24,28},{28,20},{20,12},{12,4},{4,0},{1,9},{9... | collective-permute-start | bytes 3145736 | tf_op jit(solution)/shard_map/ppermute | solution.py:259
  114.4 44.2 %collective-permute-start.27 = (f16[2,512,512]{2,1,0:T(8,128)(2,1)}, f16[2,512,512]{2,1,0:T(8,128)(2,1)S(1)}, u32[]{:S(2)}, u32[]{:S(2)}) collective-permute-start(f16[2,512,512]{2,1,0:T(8,128)(2,1)} %collective-permute-done.26), channel_id=1, source_target_pairs={{8,0},{16,8},{24,16},{28,24},{20,28},{12,20},{4,12},{0,4},{9,1},{1... | collective-permute-start | bytes 3145736 | tf_op jit(solution)/shard_map/ppermute | solution.py:260
  130.5 11.3 %collective-permute-start.17 = (f16[2,32,512]{2,1,0:T(8,128)(2,1)S(1)}, f16[2,32,512]{2,1,0:T(8,128)(2,1)S(1)}, u32[]{:S(2)}, u32[]{:S(2)}) collective-permute-start(f16[2,32,512]{2,1,0:T(8,128)(2,1)S(1)} %fusion.29), channel_id=1, source_target_pairs={{0,8},{4,12},{8,0},{12,4},{16,24},{20,28},{24,16},{28,20},{1,9},{5... | collective-permute-start | bytes 196616 | tf_op jit(solution)/shard_map/ppermute | solution.py:67
  132.3 11.1 %collective-permute-start.18 = (f16[2,32,512]{2,1,0:T(8,128)(2,1)S(1)}, f16[2,32,512]{2,1,0:T(8,128)(2,1)S(1)}, u32[]{:S(2)}, u32[]{:S(2)}) collective-permute-start(f16[2,32,512]{2,1,0:T(8,128)(2,1)S(1)} %fusion.29), channel_id=1, source_target_pairs={{0,16},{4,20},{8,24},{12,28},{16,0},{20,4},{24,8},{28,12},{1,17},{... | collective-permute-start | bytes 196616 | tf_op jit(solution)/shard_map/ppermute | solution.py:67
  134.8 11.0 %collective-permute-start.19 = (f16[2,32,512]{2,1,0:T(8,128)(2,1)S(1)}, f16[2,32,512]{2,1,0:T(8,128)(2,1)S(1)}, u32[]{:S(2)}, u32[]{:S(2)}) collective-permute-start(f16[2,32,512]{2,1,0:T(8,128)(2,1)S(1)} %fusion.29), channel_id=1, source_target_pairs={{0,24},{4,28},{8,16},{12,20},{16,8},{20,12},{24,0},{28,4},{1,25},{... | collective-permute-start | bytes 196616 | tf_op jit(solution)/shard_map/ppermute | solution.py:67
  161.7 11.7 %collective-permute-start.28 = (f16[512,512]{1,0:T(8,128)(2,1)S(1)}, f16[512,512]{1,0:T(8,128)(2,1)S(1)}, u32[]{:S(2)}, u32[]{:S(2)}) collective-permute-start(f16[512,512]{1,0:T(8,128)(2,1)S(1)} %slice_bitcast_fusion.9), channel_id=1, source_target_pairs={{8,0},{16,8},{24,16},{28,24},{20,28},{12,20},{4,12},{0,4},{9,1},{1... | collective-permute-start | bytes 1572872 | tf_op jit(solution)/shard_map/ppermute | solution.py:263
  162.7 11.8 %collective-permute-start.24 = (f16[512,512]{1,0:T(8,128)(2,1)S(1)}, f16[512,512]{1,0:T(8,128)(2,1)S(1)}, u32[]{:S(2)}, u32[]{:S(2)}) collective-permute-start(f16[512,512]{1,0:T(8,128)(2,1)S(1)} %slice_bitcast_fusion.15), channel_id=1, source_target_pairs={{0,8},{8,16},{16,24},{24,28},{28,20},{20,12},{12,4},{4,0},{1,9},{9... | collective-permute-start | bytes 1572872 | tf_op jit(solution)/shard_map/ppermute | solution.py:262
  (43 other events, 301.7 us)
